TPU v7x, 256 devices: a whole 4x4x8 slice. The times are simulated.
256 devices in a mesh: sp: 16 (over y, x), tp: 16 (over z, core).
Axes of the slice: x: 4, y: 4, z: 8, core: 2. Of those that a mesh axis runs over, the one named last changes fastest.
Arguments:
- saved_input: bfloat16 [4096, 2048], P('sp'), may hold values from -6 to 6
- cotangent: bfloat16 [4096, 2048], P('sp'), may hold values from -6 to 6
- expert_ids: int32 [4096, 2], P('sp'), may hold values from 0 to 15, all different within a row; in each aligned block of 256 rows (0 to 255, 256 to 511, ...) at most 64 rows name the same one
- route_weight: float32 [4096, 2], P('sp'), may hold values from 0.1 to 0.9
- w_gate: bfloat16 [16, 2048, 6144], P('sp', None, 'tp'), may hold values from -0.125 to 0.125
- w_up: bfloat16 [16, 2048, 6144], P('sp', None, 'tp'), may hold values from -0.125 to 0.125
- w_down: bfloat16 [16, 6144, 2048], P('sp', 'tp'), may hold values from -0.078125 to 0.078125
- w_out: bfloat16 [2048, 2048], P(None, 'tp'), may hold values from -0.125 to 0.125
- channel_gain: float32 [2048], P('tp'), may hold values from 0.1 to 1.9
- conv_taps: float32 [31, 2048], P(None, 'tp'), may hold values from -1 to 1
- glu_value: bfloat16 [2048, 4096], P('tp', 'sp'), may hold values from -6 to 6
- glu_gate: bfloat16 [2048, 4096], P('tp', 'sp'), may hold values from -8 to 8
- conv_out: bfloat16 [2048, 4096], P('tp', 'sp'), may hold values from -6 to 6
- norm_mean: float32 [4096], P('sp'), may hold values from -3 to 3
- norm_rstd: float32 [4096], P('sp'), may hold values from 0.5 to 2
Outputs:
- gate_grad: bfloat16 [16, 2048, 6144], P('sp', None, 'tp')
- up_grad: bfloat16 [16, 2048, 6144], P('sp', None, 'tp')
- down_grad: bfloat16 [16, 6144, 2048], P('sp', 'tp')
- proj_grad: float32 [2048, 2048], P('sp', 'tp')
- value_grad: bfloat16 [2048, 4096], P('tp', 'sp')
- gate_in_grad: bfloat16 [2048, 4096], P('tp', 'sp')
Inputs may be any that keep to these rules, and one draw needn't show every extreme that they name: `expert_ids`: the two experts of a position differ. In the positions of one block of 256, no expert is named more than 64 times, a bound that some block reaches.
All inputs are finite; a program needn't handle non-finite values.
Results may differ from a plain program's by a relative error of at most 0.018.
Values may be sent and summed in bfloat16 or wider, within the bound.
No kernel may reach another device: no remote copies, remote signals or barrier semaphores. Data moves between devices by JAX's collectives and lax.ppermute only.
A program may use at most 128 MiB of HBM per device.

v0:
```python
import jax
import jax.numpy as jnp
from jax import lax
from jax.sharding import PartitionSpec as P

D = 2048
C = 2048


def in_one_piece(arrays, axis, split_dim, concat_dim, along):
    ends, at = ([], 0)
    for a in arrays[:-1]:
        at += a.shape[along]
        ends.append(at)
    both = jnp.concatenate(arrays, axis=along)
    return tuple(
        jnp.split(
            lax.all_to_all(both, axis, split_axis=split_dim, concat_axis=concat_dim, tiled=True),
            ends,
            axis=along,
        )
    )


def cut_along(value, dim, devices):
    before, after = (value.shape[:dim], value.shape[dim + 1 :])
    return jnp.moveaxis(value.reshape(*before, devices, -1, *after), dim, 0)


def sent_and_summed(value, axis, dim):
    devices = lax.axis_size(axis)
    tiles = lax.all_to_all(cut_along(value, dim, devices), axis, 0, 0, tiled=True)
    return jnp.sum(tiles.astype(jnp.float32), axis=0)


def copy_for_each(value, axis):
    copies = jnp.broadcast_to(value, (lax.axis_size(axis), *value.shape))
    return lax.all_to_all(copies, axis, split_axis=0, concat_axis=0, tiled=True)


def of_everyone(value, axis):
    everything = copy_for_each(value, axis)
    return jnp.sum(everything, axis=0)


def in_one(arrays, axis):
    ravelled, at, gathered = (jnp.concatenate([a.reshape(-1) for a in arrays]), 0, [])
    subtotal = of_everyone(ravelled, axis)
    for a in arrays:
        gathered.append(subtotal[at : at + a.size].reshape(a.shape))
        at += a.size
    return tuple(gathered)


def from_behind(value, axis, by):
    devices = lax.axis_size(axis)
    pairs = [(i, i + by) for i in range(devices) if 0 <= i + by < devices]
    return lax.ppermute(value, axis, pairs)


def contract(left, right, left_dim, right_dim):
    return lax.dot_general(
        left, right, (((left_dim,), (right_dim,)), ((), ())), preferred_element_type=jnp.float32
    )


def expert_grads(rows_in, rows_cot, gate_weight, up_weight, down_weight):
    gate_pre = jnp.dot(rows_in, gate_weight, preferred_element_type=jnp.float32)
    up_pre = jnp.dot(rows_in, up_weight, preferred_element_type=jnp.float32)
    sigma = jax.nn.sigmoid(gate_pre)
    hidden = (gate_pre * sigma * up_pre).astype(jnp.bfloat16)
    hidden_cot = contract(rows_cot, down_weight, 1, 1)
    down_part = contract(hidden, rows_cot, 0, 0).astype(jnp.bfloat16)
    gate_cot = (hidden_cot * up_pre * sigma * (1.0 + gate_pre * (1.0 - sigma))).astype(jnp.bfloat16)
    up_cot = (hidden_cot * gate_pre * sigma).astype(jnp.bfloat16)
    gate_part = contract(rows_in, gate_cot, 0, 0).astype(jnp.bfloat16)
    up_part = contract(rows_in, up_cot, 0, 0).astype(jnp.bfloat16)
    input_cot = contract(gate_cot, gate_weight, 1, 1) + contract(up_cot, up_weight, 1, 1)
    return (gate_part, up_part, down_part, input_cot)


def on_device(
    saved_input,
    cotangent,
    expert_ids,
    route_weight,
    w_gate,
    w_up,
    w_down,
    w_out,
    channel_gain,
    conv_taps,
    glu_value,
    glu_gate,
    conv_out,
    norm_mean,
    norm_rstd,
):
    tokens_here = cotangent.shape[0]
    sp_count = lax.axis_size("sp")
    local_experts = w_gate.shape[0]
    expert_count = local_experts * sp_count
    capacity = 4 * tokens_here // expert_count
    pairs = expert_ids.reshape(2 * tokens_here)
    onehot = (pairs[:, None] == jnp.arange(expert_count, dtype=jnp.int32)[None, :]).astype(
        jnp.int32
    )
    before = jnp.cumsum(onehot, axis=0) - onehot
    target = pairs * capacity + jnp.sum(before * onehot, axis=1)
    owner = (
        jnp.zeros((expert_count * capacity,), jnp.int32)
        .at[target]
        .set(jnp.arange(2 * tokens_here, dtype=jnp.int32) + 1)
    )
    filled = (owner > 0)[:, None]
    pair_index = jnp.maximum(owner - 1, 0)
    scaled = (route_weight[:, :, None] * cotangent.astype(jnp.float32)[:, None, :]).astype(
        jnp.bfloat16
    )
    scaled = scaled.reshape(2 * tokens_here, D)
    send_cot = jnp.where(filled, scaled[pair_index], jnp.zeros_like(scaled[:1])).reshape(
        expert_count, capacity, D
    )
    send_in = jnp.where(filled, saved_input[pair_index // 2], jnp.zeros_like(saved_input[:1]))
    send_in = send_in.reshape(expert_count, capacity, D)
    rows_cot, rows_in = in_one_piece((send_cot, send_in), "sp", 0, 1, 2)
    results = [expert_grads(rows_in[0], rows_cot[0], w_gate[0], w_up[0], w_down[0])]
    gate_grad = jnp.stack([result[0] for result in results])
    up_grad = jnp.stack([result[1] for result in results])
    down_grad = jnp.stack([result[2] for result in results])
    input_cot = jnp.stack([result[3] for result in results])
    blocks = input_cot.reshape(local_experts, sp_count, capacity, D)
    share = lax.psum_scatter(
        blocks.astype(jnp.bfloat16), "tp", scatter_dimension=2, tiled=True
    ).astype(jnp.float32)
    returned = lax.all_to_all(
        share.astype(jnp.bfloat16), "sp", split_axis=1, concat_axis=0, tiled=True
    ).astype(share.dtype)
    whole = lax.all_gather(returned.astype(jnp.bfloat16), "tp", axis=2, tiled=True).astype(
        returned.dtype
    )
    routed = whole.reshape(expert_count * capacity, D)[target].reshape(tokens_here, 2, D)
    summed = jnp.sum(routed, axis=1)
    mixed_cot = (cotangent.astype(jnp.float32) + summed).astype(jnp.bfloat16)
    centered = (conv_out.astype(jnp.float32) - norm_mean[None, :]) * norm_rstd[None, :]
    normed = centered * channel_gain[:, None]
    sigma = jax.nn.sigmoid(normed)
    output_act = (normed * sigma).astype(jnp.bfloat16)
    proj_grad = sent_and_summed(contract(mixed_cot, output_act, 0, 1).astype(jnp.bfloat16), "sp", 0)
    act_cot = contract(w_out, mixed_cot, 0, 1)
    norm_cot = act_cot * sigma * (1.0 + normed * (1.0 - sigma)) * channel_gain[:, None]
    first_sum, second_sum = in_one(
        (jnp.sum(norm_cot, axis=0), jnp.sum(norm_cot * centered, axis=0)), "tp"
    )
    conv_cot = norm_rstd[None, :] * (
        norm_cot - first_sum[None, :] / C - centered * second_sum[None, :] / C
    )
    reach = conv_taps.shape[0] - 1
    rim = from_behind(conv_cot[:, :reach], "sp", -1)
    padded = jnp.concatenate([conv_cot, rim], axis=1)
    glu_cot = conv_taps[0][:, None] * padded[:, :tokens_here]
    for lag in range(1, reach + 1):
        glu_cot = glu_cot + conv_taps[lag][:, None] * padded[:, lag : lag + tokens_here]
    gate_sigma = jax.nn.sigmoid(glu_gate.astype(jnp.float32))
    value_grad = (glu_cot * gate_sigma).astype(jnp.bfloat16)
    gate_in_grad = (
        glu_cot * glu_value.astype(jnp.float32) * gate_sigma * (1.0 - gate_sigma)
    ).astype(jnp.bfloat16)
    return (gate_grad, up_grad, down_grad, proj_grad, value_grad, gate_in_grad)


def solution(mesh):
    in_specs = (
        P("sp", None),
        P("sp", None),
        P("sp", None),
        P("sp", None),
        P("sp", None, "tp"),
        P("sp", None, "tp"),
        P("sp", "tp", None),
        P(None, "tp"),
        P("tp"),
        P(None, "tp"),
        P("tp", "sp"),
        P("tp", "sp"),
        P("tp", "sp"),
        P("sp"),
        P("sp"),
    )
    out_specs = (
        P("sp", None, "tp"),
        P("sp", None, "tp"),
        P("sp", "tp", None),
        P("sp", "tp"),
        P("tp", "sp"),
        P("tp", "sp"),
    )
    return jax.shard_map(
        on_device, mesh=mesh, in_specs=in_specs, out_specs=out_specs, check_vma=False
    )
```

profile of v0, /device:TPU:24, one launch (start us, length us, event | category | flops | bytes accessed | tf_op | source)
XLA Modules:
  0.0 370.5 jit_solution(13635867785435302561)
XLA Ops:
  7.2 0.8 broadcast_multiply_fusion
  8.0 0.8 copy.65
  8.8 0.1 eq.25
  9.3 0.1 mul.436
  9.4 1.2 reduce-window.6
  10.6 0.2 slice_reduce_fusion
  11.0 2.4 scatter_custom_fusion
  13.5 5.3 %mul.440 = f32[256,2,2048]{2,1,0:T(2,128)} broadcast(bf16[256,2048]{1,0:T(8,128)(2,1)} %param.16), dimensions={0,2} | broadcast | bytes 5242880 | tf_op jit(solution)/shard_map/mul | solution.py:117
  18.8 6.1 %mul.441 = f32[512,2048]{1,0:T(8,128)} reshape(f32[256,2,2048]{2,1,0:T(2,128)} %mul.440) | data formatting | bytes 8388608 | tf_op jit(solution)/shard_map/mul | solution.py:117
  25.0 0.1 mul.438
  25.2 3.8 %multiply_convert_fusion = bf16[512,2048]{1,0:T(8,128)(2,1)} fusion(f32[512,2048]{1,0:T(8,128)} %mul.441, f32[512]{0:T(512)S(1)} %mul.438), kind=kLoop, calls=%fused_computation.8 | loop fusion | flops 2097152 | bytes 6293504 | tf_op jit(solution)/shard_map/convert_element_type | solution.py:117
  29.0 10.8 %gather_fusion = bf16[1024,2048]{1,0:T(8,128)(2,1)} fusion(bf16[512,2048]{1,0:T(8,128)(2,1)} %multiply_convert_fusion, s32[1024]{0:T(1024)S(1)} %get-tuple-element.73), kind=kCustom, calls=%fused_computation | custom fusion | bytes 8392704 | tf_op jit(solution)/shard_map/gather | solution.py:121
  39.8 6.0 %gather_fusion.1 = bf16[1024,2048]{1,0:T(8,128)(2,1)} fusion(bf16[256,2048]{1,0:T(8,128)(2,1)S(1)} %copy-done.2, s32[1024]{0:T(1024)S(1)} %get-tuple-element.74), kind=kCustom, calls=%fused_computation.1 | custom fusion | bytes 8392704 | tf_op jit(solution)/shard_map/gather | solution.py:124
  45.8 5.8 %broadcast_select_fusion.1 = (bf16[16,64,2048]{2,1,0:T(8,128)(2,1)}, bf16[16,64,2048]{2,1,0:T(8,128)(2,1)}) fusion(bf16[16,64,2048]{2,1,0:T(8,128)(2,1)} %bitcast.144, pred[16,64]{1,0:T(8,128)(4,1)S(1)} %broadcast_in_dim.46, bf16[16,64,2048]{2,1,0:T(8,128)(2,1)} %bitcast.145), kind=kLoop, calls=%fused_computation.10 | loop fusion | flops 4194304 | bytes 16778240 | tf_op jit(solution)/shard_map/jit(_where)/select_n | solution.py:121
  51.6 7.8 %pad_maximum_fusion = bf16[16,64,4096]{2,1,0:T(8,128)(2,1)} fusion(bf16[16,64,2048]{2,1,0:T(8,128)(2,1)} %get-tuple-element.78, bf16[16,64,2048]{2,1,0:T(8,128)(2,1)} %get-tuple-element.77), kind=kLoop, calls=%fused_computation.4 | loop fusion | flops 16777216 | bytes 16777216 | tf_op jit(solution)/shard_map/concatenate | solution.py:15
  59.4 100.8 %all_to_all.35 = bf16[16,64,4096]{2,1,0:T(8,128)(2,1)S(1)} all-to-all(bf16[16,64,4096]{2,1,0:T(8,128)(2,1)} %pad_maximum_fusion), channel_id=1, replica_groups=mesh['sp'=16,'tp'=16] {'sp'}, dimensions={0} | all-to-all | bytes 16777216 | tf_op jit(solution)/shard_map/all_to_all | solution.py:18
  160.3 2.3 fusion.3
  162.6 0.2 copy-done.5
  162.8 2.3 fusion.4
  165.2 0.2 copy-done.15
  165.4 2.8 multiply_convert_fusion.2
  168.2 2.4 fusion.8
  170.6 2.4 add_convert_fusion
  173.0 4.3 %copy.69 = bf16[1,16,64,2048]{3,1,0,2:T(8,128)(2,1)} copy(bf16[1,16,64,2048]{3,2,1,0:T(8,128)(2,1)S(1)} %bitcast.146) | data formatting | bytes 8388608 | tf_op jit(solution)/shard_map/convert_element_type | solution.py:134
  177.3 64.5 %reduce-scatter.2.cloned.1.call-done = bf16[1,16,4,2048]{3,1,0,2:T(8,128)(2,1)} async-done(((bf16[1,16,64,2048]{3,1,0,2:T(8,128)(2,1)}), bf16[1,16,4,2048]{3,1,0,2:T(8,128)(2,1)}) %reduce-scatter.2.cloned.1.call-update) | async-done | bytes 262160 | tf_op jit(solution)/shard_map/reduce_scatter | solution.py:133
  241.9 1.2 copy.70
  243.0 13.6 %all_to_all.36 = bf16[1,16,4,2048]{3,2,0,1:T(4,128)(2,1)S(1)} all-to-all(bf16[1,16,4,2048]{3,2,0,1:T(4,128)(2,1)S(1)} %copy.70), channel_id=1, replica_groups=mesh['sp'=16,'tp'=16] {'sp'}, dimensions={1} | all-to-all | bytes 524288 | tf_op jit(solution)/shard_map/all_to_all | solution.py:136
  256.6 0.9 copy.71
  258.0 5.9 %fusion.5 = bf16[1,2048,384]{2,1,0:T(8,128)(2,1)} fusion(bf16[1024,384]{1,0:T(8,128)(2,1)S(1)} %get-tuple-element.41, bf16[1,1024,4096]{2,1,0:T(8,128)(2,1)} %bitcast.150), kind=kOutput, calls=%fused_computation.18 | convolution fusion | flops 1611399168 | bytes 6553600 | tf_op jit(solution)/shard_map/dot_general | solution.py:62
  263.9 5.4 %fusion.7 = bf16[1,384,2048]{2,1,0:T(8,128)(2,1)} fusion(bf16[1,1024,4096]{2,1,0:T(8,128)(2,1)} %bitcast.151, f32[1024,384]{1,0:T(8,128)S(1)} %copy-done.19, f32[1024,384]{1,0:T(8,128)S(1)} %copy-done.17), kind=kOutput, calls=%fused_computation.20 | convolution fusion | flops 1613758464 | bytes 8912896 | tf_op jit(solution)/shard_map/dot_general | solution.py:62
  269.3 26.8 %all-gather.3.cloned.1.call-done = bf16[1,16,64,2048]{3,1,0,2:T(8,128)(2,1)} async-done(((bf16[1,16,4,2048]{3,1,0,2:T(8,128)(2,1)}), bf16[1,16,64,2048]{3,1,0,2:T(8,128)(2,1)}) %all-gather.3.cloned.1.call-update) | async-done | bytes 4194320 | tf_op jit(solution)/shard_map/all_gather | solution.py:139
  296.1 7.8 %copy.72 = f32[1,16,64,2048]{3,2,1,0:T(8,128)} copy(bf16[1,16,64,2048]{3,1,0,2:T(8,128)(2,1)} %all-gather.3.cloned.1.call-done) | data formatting | bytes 12582912 | tf_op jit(solution)/shard_map/reshape | solution.py:142
  303.9 8.8 %gather_fusion.2 = f32[512,2048]{1,0:T(8,128)} fusion(f32[1024,2048]{1,0:T(8,128)} %bitcast.143, s32[1024]{0:T(1024)S(1)} %pad_clamp_fusion), kind=kCustom, calls=%fused_computation.2 | custom fusion | bytes 8390656 | tf_op jit(solution)/shard_map/gather | solution.py:142
  312.7 6.1 %reshape.159 = f32[256,2,2048]{2,1,0:T(2,128)} reshape(f32[512,2048]{1,0:T(8,128)} %gather_fusion.2) | data formatting | bytes 8388608 | tf_op jit(solution)/shard_map/reshape | solution.py:142
  318.8 8.6 %reduce_sum.58 = f32[256,2048]{1,0:T(8,128)} reduce(f32[256,2,2048]{2,1,0:T(2,128)} %reshape.159, f32[]{:T(128)} %constant.44.clone.1), dimensions={1}, to_apply=%region_5.6 | reduce | flops 524288 | bytes 6291460 | tf_op jit(solution)/shard_map/reduce_sum | solution.py:143
  327.5 2.1 fusion.123
  329.6 0.6 broadcast_in_dim.51
  330.3 4.4 %all-to-all-start.3 = ((f32[16,1,512]{2,1,0:T(1,128)}), f32[16,1,512]{2,1,0:T(1,128)S(1)}, u32[]{:S(2)}, u32[]{:S(2)}) async-start(f32[16,1,512]{2,1,0:T(1,128)} %broadcast_in_dim.51), calls=%async_computation.4 | async-start | bytes 65536 | tf_op jit(solution)/shard_map/all_to_all | solution.py:38
  334.6 3.1 convolution_convert_fusion.2
  337.7 4.6 %all-to-all-done.3 = f32[16,1,512]{2,1,0:T(1,128)S(1)} async-done(((f32[16,1,512]{2,1,0:T(1,128)}), f32[16,1,512]{2,1,0:T(1,128)S(1)}, u32[]{:S(2)}, u32[]{:S(2)}) %all-to-all-start.3) | async-done | bytes 32800 | tf_op jit(solution)/shard_map/all_to_all | solution.py:38
  342.3 7.2 %all-to-all-start.2 = ((bf16[16,128,128]{2,1,0:T(8,128)(2,1)}), bf16[16,128,128]{2,1,0:T(8,128)(2,1)S(1)}, u32[]{:S(2)}, u32[]{:S(2)}) async-start(bf16[16,128,128]{2,1,0:T(8,128)(2,1)} %bitcast.16), calls=%async_computation.3 | async-start | bytes 1048576 | tf_op jit(solution)/shard_map/all_to_all | solution.py:32
  349.6 0.2 subtract_multiply_fusion
  349.8 4.9 %collective-permute-start = (f32[128,30]{0,1:T(8,128)S(1)}, f32[128,30]{0,1:T(8,128)S(1)}, u32[]{:S(2)}, u32[]{:S(2)}) collective-permute-start(f32[128,30]{0,1:T(8,128)S(1)} %slice.271), channel_id=1, source_target_pairs={{16,0},{32,16},{48,32},{64,48},{80,64},{96,80},{112,96},{128,112},... | collective-permute-start | bytes 46088 | tf_op jit(solution)/shard_map/ppermute | solution.py:58
  354.7 5.8 %fusion.6 = bf16[1,2048,384]{2,1,0:T(8,128)(2,1)} fusion(bf16[1024,384]{1,0:T(8,128)(2,1)S(1)} %get-tuple-element.40, bf16[1,1024,4096]{2,1,0:T(8,128)(2,1)} %bitcast.152), kind=kOutput, calls=%fused_computation.19 | convolution fusion | flops 1611399168 | bytes 6553600 | tf_op jit(solution)/shard_map/dot_general | solution.py:62
  360.5 0.4 multiply_convert_fusion.5
  361.0 0.7 copy.77
  361.8 0.7 copy.78
  362.5 0.7 convert_reduce_fusion
  (67 shorter events, 1.3 us)
Async XLA Ops:
  7.2 153.1 %copy-start = (bf16[1,2048,384]{2,1,0:T(8,128)(2,1)S(1)}, bf16[1,2048,384]{2,1,0:T(8,128)(2,1)}, u32[]{:S(2)}) copy-start(bf16[1,2048,384]{2,1,0:T(8,128)(2,1)} %param.19) | copy-start | bytes 4718596
  7.2 234.7 %reduce-scatter.2.cloned.1.call-start = ((), (), s32[]{:S(2)}) async-start(), calls=%async_computation.5 | async-start | bytes 4456448 | tf_op jit(solution)/shard_map/reduce_scatter | solution.py:133
  18.8 6.1 %copy-start.13 = (f32[256,2]{0,1:T(2,128)S(1)}, f32[256,2]{0,1:T(2,128)}, u32[]{:S(2)}) copy-start(f32[256,2]{0,1:T(2,128)} %param.18) | copy-start | bytes 6148
  29.0 10.8 %copy-start.2 = (bf16[256,2048]{1,0:T(8,128)(2,1)S(1)}, bf16[256,2048]{1,0:T(8,128)(2,1)}, u32[]{:S(2)}) copy-start(bf16[256,2048]{1,0:T(8,128)(2,1)} %param.15) | copy-start | bytes 3145732
  160.3 4.9 %copy-start.4 = (bf16[16,64,4096]{2,1,0:T(8,128)(2,1)}, bf16[16,64,4096]{2,1,0:T(8,128)(2,1)S(1)}, u32[]{:S(2)}) copy-start(bf16[16,64,4096]{2,1,0:T(8,128)(2,1)S(1)} %all_to_all.35) | copy-start | bytes 25165828
  160.3 2.6 copy-start.5
  162.8 2.4 copy-start.16
  162.8 2.6 copy-start.15
  165.4 2.8 copy-start.18
  177.3 80.3 %copy-start.7 = (bf16[128,256]{1,0:T(8,128)(2,1)S(1)}, bf16[128,256]{1,0:T(8,128)(2,1)}, u32[]{:S(2)}) copy-start(bf16[128,256]{1,0:T(8,128)(2,1)} %param.27) | copy-start | bytes 196612
  177.3 80.4 %copy-start.8 = (bf16[128,256]{1,0:T(8,128)(2,1)S(1)}, bf16[128,256]{1,0:T(8,128)(2,1)}, u32[]{:S(2)}) copy-start(bf16[128,256]{1,0:T(8,128)(2,1)} %param.25) | copy-start | bytes 196612
  177.3 80.5 %copy-start.9 = (bf16[128,256]{1,0:T(8,128)(2,1)S(1)}, bf16[128,256]{1,0:T(8,128)(2,1)}, u32[]{:S(2)}) copy-start(bf16[128,256]{1,0:T(8,128)(2,1)} %param.26) | copy-start | bytes 196612
  177.3 80.7 %copy-start.10 = (f32[31,128]{1,0:T(8,128)S(1)}, f32[31,128]{1,0:T(8,128)}, u32[]{:S(2)}) copy-start(f32[31,128]{1,0:T(8,128)} %param.24) | copy-start | bytes 47620
  177.3 118.8 %all-gather.3.cloned.1.call-start = ((), (), s32[]{:S(2)}) async-start(), calls=%async_computation.6 | async-start | bytes 4456448 | tf_op jit(solution)/shard_map/all_gather | solution.py:139
  258.0 5.9 %copy-start.17 = (f32[1024,384]{1,0:T(8,128)S(1)}, f32[1024,384]{1,0:T(8,128)}, u32[]{:S(2)}) copy-start(f32[1024,384]{1,0:T(8,128)} %copy-done.16) | copy-start | bytes 4718596
  258.0 5.9 %copy-start.19 = (f32[1024,384]{1,0:T(8,128)S(1)}, f32[1024,384]{1,0:T(8,128)}, u32[]{:S(2)}) copy-start(f32[1024,384]{1,0:T(8,128)} %copy-done.18) | copy-start | bytes 4718596
  318.7 8.7 %copy-start.3 = (bf16[256,2048]{1,0:T(8,128)(2,1)S(1)}, bf16[256,2048]{1,0:T(8,128)(2,1)}, u32[]{:S(2)}) copy-start(bf16[256,2048]{1,0:T(8,128)(2,1)} %param.16) | copy-start | bytes 3145732
  318.8 8.7 %copy-start.6 = (bf16[2048,128]{1,0:T(8,128)(2,1)S(1)}, bf16[2048,128]{1,0:T(8,128)(2,1)}, u32[]{:S(2)}) copy-start(bf16[2048,128]{1,0:T(8,128)(2,1)} %param.22) | copy-start | bytes 1572868
  318.8 8.7 %copy-start.11 = (f32[256]{0:T(256)S(1)}, f32[256]{0:T(256)}, u32[]{:S(2)}) copy-start(f32[256]{0:T(256)} %param.29) | copy-start | bytes 3076
  318.8 8.7 %copy-start.12 = (f32[256]{0:T(256)S(1)}, f32[256]{0:T(256)}, u32[]{:S(2)}) copy-start(f32[256]{0:T(256)} %param.28) | copy-start | bytes 3076
  318.8 8.7 %copy-start.14 = (f32[128]{0:T(128)S(1)}, f32[128]{0:T(128)}, u32[]{:S(2)}) copy-start(f32[128]{0:T(128)} %param.23) | copy-start | bytes 1540
  330.3 12.1 %all-to-all-start.3 = ((f32[16,1,512]{2,1,0:T(1,128)}), f32[16,1,512]{2,1,0:T(1,128)S(1)}, u32[]{:S(2)}, u32[]{:S(2)}) async-start(f32[16,1,512]{2,1,0:T(1,128)} %broadcast_in_dim.51), calls=%async_computation.4 | async-start | bytes 65536 | tf_op jit(solution)/shard_map/all_to_all | solution.py:38
  342.3 20.2 %all-to-all-start.2 = ((bf16[16,128,128]{2,1,0:T(8,128)(2,1)}), bf16[16,128,128]{2,1,0:T(8,128)(2,1)S(1)}, u32[]{:S(2)}, u32[]{:S(2)}) async-start(bf16[16,128,128]{2,1,0:T(8,128)(2,1)} %bitcast.16), calls=%async_computation.3 | async-start | bytes 1048576 | tf_op jit(solution)/shard_map/all_to_all | solution.py:32
  349.8 10.7 %collective-permute-start = (f32[128,30]{0,1:T(8,128)S(1)}, f32[128,30]{0,1:T(8,128)S(1)}, u32[]{:S(2)}, u32[]{:S(2)}) collective-permute-start(f32[128,30]{0,1:T(8,128)S(1)} %slice.271), channel_id=1, source_target_pairs={{16,0},{32,16},{48,32},{64,48},{80,64},{96,80},{112,96},{128,112},... | collective-permute-start | bytes 46088 | tf_op jit(solution)/shard_map/ppermute | solution.py:58
  354.7 8.5 %copy-start.1 = (bf16[1,2048,384]{2,1,0:T(8,128)(2,1)S(1)}, bf16[1,2048,384]{2,1,0:T(8,128)(2,1)}, u32[]{:S(2)}) copy-start(bf16[1,2048,384]{2,1,0:T(8,128)(2,1)} %param.19) | copy-start | bytes 4718596
Sparse Core Ops, SparseCore 0:
  177.4 64.3 reduce-scatter.1
  257.6 38.3 all-gather.2
where the time goes:
time: 377 us; the launch traced here: 370 us
  blocking collectives  114 us (30%)
  waiting for transfers between devices  95.9 us (25%)
  local copies, waits for them, and re-layouts  64.6 us (17%)
  matrix products  34.5 us (9%)
  other arithmetic  29.5 us (8%)
  starting transfers between devices  16.5 us (4%)
  between operations  14.9 us (4%)
    all_to_all x1, blocking collectives, in_one_piece(): lax.all_to_all(both, axis, split_axis=split_dim, concat_axis=concat_dim,...  101 us
    reduce_scatter x1, waiting for transfers between devices, on_device(): lax.psum_scatter(blocks.astype(jnp.bfloat16), 'tp', scatter_dimension=2,...  64.5 us
    dot_general x8, matrix products, contract(): lax.dot_general(left, right, (((left_dim,), (right_dim,)), ((), ())), pre...  29.9 us
    all_gather x1, waiting for transfers between devices, on_device(): lax.all_gather(returned.astype(jnp.bfloat16), 'tp', axis=2, tiled=True)  26.8 us
    reshape x2, local copies, waits for them, and re-layouts, on_device(): whole.reshape(expert_count * capacity, D)[target].reshape(tokens_here, 2, D)  13.9 us
    all_to_all x1, blocking collectives, on_device(): lax.all_to_all(share.astype(jnp.bfloat16), 'sp', split_axis=1, concat_axi...  13.6 us
    mul x3, local copies, waits for them, and re-layouts, on_device(): route_weight[:, :, None] * cotangent.astype(jnp.float32)[:, None, :]  11.6 us
    gather x1, local copies, waits for them, and re-layouts, on_device(): scaled[pair_index]  10.8 us
  transfers between devices with their start and end apart: 5, of which 3 were waited for; matrix products, arithmetic and copies ran while one was open for 6% of the time, Pallas kernels for 0%

commit v1 on v0

v1 whole, which is shorter than its diff:
```python
import functools

import jax
import jax.numpy as jnp
from jax import lax
from jax.experimental import pallas as pl
from jax.experimental.pallas import tpu as pltpu
from jax.sharding import PartitionSpec as P


D = 2048
C = 2048
HALF = D // 2
BF = jnp.bfloat16
F32 = jnp.float32


def contract(left, right, left_dim, right_dim):
    return lax.dot_general(
        left, right, (((left_dim,), (right_dim,)), ((), ())), preferred_element_type=F32
    )


def exchanged(value, axis, groups=None):
    return lax.all_to_all(value, axis, 0, 0, axis_index_groups=groups, tiled=True)


def swapped_cores(value):
    pairs = [(i, i ^ 1) for i in range(lax.axis_size("tp"))]
    return lax.ppermute(value, "tp", pairs)


def small_vmem():
    return pltpu.CompilerParams(vmem_limit_bytes=6 * 1024 * 1024)


def in_vmem(count):
    return [pl.BlockSpec(memory_space=pltpu.VMEM)] * count


SCALAR = pl.BlockSpec(memory_space=pltpu.SMEM)


def route_kernel(pairs, saved_input, cotangent, sent, target, *, experts, slots):
    tokens = pairs.shape[1]
    ids = pairs[0:2, :].astype(jnp.int32)
    weights = pairs[2:4, :]
    expert = lax.broadcasted_iota(jnp.int32, (experts, tokens), 0)
    first = ids[0:1, :] == expert
    second = ids[1:2, :] == expert
    named = jnp.where(first | second, 1.0, 0.0).astype(BF)
    earlier = lax.broadcasted_iota(jnp.int32, (tokens, tokens), 0) < lax.broadcasted_iota(
        jnp.int32, (tokens, tokens), 1
    )
    count = jnp.dot(named, jnp.where(earlier, 1.0, 0.0).astype(BF), preferred_element_type=F32)
    places = []
    for k, chosen in ((0, first), (1, second)):
        slot = jnp.sum(jnp.where(chosen, count, 0.0), axis=0, keepdims=True)
        places.append(ids[k : k + 1, :] * slots + slot.astype(jnp.int32))
    across = jnp.concatenate(places + [jnp.zeros((6, tokens), jnp.int32)], axis=0)
    target[...] = across.astype(F32).T[:, 0:2].astype(jnp.int32)

    rows = 256
    for step in range(experts * slots // rows):
        row = lax.broadcasted_iota(jnp.int32, (rows, tokens), 0) + step * rows
        hit0 = row == places[0]
        hit1 = row == places[1]
        select = jnp.where(hit0 | hit1, 1.0, 0.0).astype(BF)
        weight = jnp.sum(
            jnp.where(hit0, weights[0:1, :], 0.0) + jnp.where(hit1, weights[1:2, :], 0.0),
            axis=1,
            keepdims=True,
        )
        here = slice(step * rows, (step + 1) * rows)
        moved_in = jnp.dot(select, saved_input[...], preferred_element_type=F32)
        sent[here, :HALF] = moved_in.astype(BF)
        moved = jnp.dot(select, cotangent[...], preferred_element_type=F32)
        sent[here, HALF:] = (moved * weight).astype(BF)


def routed(pairs, half_in, half_cot, experts, slots):
    tokens = pairs.shape[1]
    return pl.pallas_call(
        functools.partial(route_kernel, experts=experts, slots=slots),
        in_specs=in_vmem(3),
        out_specs=in_vmem(2),
        out_shape=[
            jax.ShapeDtypeStruct((experts * slots, D), BF),
            jax.ShapeDtypeStruct((tokens, 2), jnp.int32),
        ],
        compiler_params=small_vmem(),
        name="route",
    )(pairs, half_in, half_cot)


ROWS = 256


def half_of(core, flip):
    index = 1 - core[0] if flip else core[0]
    return pl.ds(pl.multiple_of(index * HALF, HALF), HALF)


def own_kernel(core, own, w_gate, w_up, w_down, first_part, cot_part, pair_own, pair_other):
    units = w_gate.shape[1]
    half, far = half_of(core, False), half_of(core, True)
    pair_own[:, :units] = w_gate[half, :]
    pair_own[:, units:] = w_up[half, :]
    for step in range(own.shape[0] // ROWS):
        here = slice(step * ROWS, (step + 1) * ROWS)
        first_part[here, :] = contract(own[here, :HALF], pair_own[...], 1, 0)
        cot_part[here, :] = contract(own[here, HALF:], w_down[:, half], 1, 1)
    pair_other[:, :units] = w_gate[far, :]
    pair_other[:, units:] = w_up[far, :]


def own_products(core, own, w_gate, w_up, w_down):
    total, units = own.shape[0], w_gate.shape[1]
    return pl.pallas_call(
        own_kernel,
        in_specs=[SCALAR] + in_vmem(4),
        out_specs=in_vmem(4),
        out_shape=[
            jax.ShapeDtypeStruct((total, 2 * units), F32),
            jax.ShapeDtypeStruct((total, units), F32),
            jax.ShapeDtypeStruct((HALF, 2 * units), BF),
            jax.ShapeDtypeStruct((HALF, 2 * units), BF),
        ],
        compiler_params=small_vmem(),
        name="own_products",
    )(core, own, w_gate, w_up, w_down)


def other_kernel(
    core, other, first_part, cot_part, pair_other, w_down, hidden_out, cots, send,
):
    half = half_of(core, True)
    units = w_down.shape[0]
    for step in range(other.shape[0] // ROWS):
        here = slice(step * ROWS, (step + 1) * ROWS)
        first = first_part[here, :] + contract(other[here, :HALF], pair_other[...], 1, 0)
        gate_pre, up_pre = first[:, :units], first[:, units:]
        hidden_cot = cot_part[here, :] + contract(other[here, HALF:], w_down[:, half], 1, 1)
        sigma = jax.nn.sigmoid(gate_pre)
        silu = gate_pre * sigma
        hidden_out[here, :] = (silu * up_pre).astype(BF)
        cots[here, :units] = (
            hidden_cot * up_pre * sigma * (1.0 + gate_pre * (1.0 - sigma))
        ).astype(BF)
        cots[here, units:] = (hidden_cot * silu).astype(BF)
        send[here, :] = contract(cots[here, :], pair_other[...], 1, 1).astype(BF)


def other_products(core, other, first_part, cot_part, pair_other, w_down):
    total, units = other.shape[0], w_down.shape[0]
    return pl.pallas_call(
        other_kernel,
        in_specs=[SCALAR] + in_vmem(5),
        out_specs=in_vmem(3),
        out_shape=[
            jax.ShapeDtypeStruct((total, units), BF),
            jax.ShapeDtypeStruct((total, 2 * units), BF),
            jax.ShapeDtypeStruct((total, HALF), BF),
        ],
        compiler_params=small_vmem(),
        name="other_products",
    )(core, other, first_part, cot_part, pair_other, w_down)


def keep_kernel(cots, pair_own, hidden, keep, hidden_t):
    for step in range(keep.shape[0] // ROWS):
        here = slice(step * ROWS, (step + 1) * ROWS)
        keep[here, :] = contract(cots[here, :], pair_own[...], 1, 1).astype(BF)
    hidden_t[...] = hidden[...].T


def kept_half(cots, pair_own, hidden):
    total, units = hidden.shape
    return pl.pallas_call(
        keep_kernel,
        in_specs=in_vmem(3),
        out_specs=in_vmem(2),
        out_shape=[
            jax.ShapeDtypeStruct((total, HALF), BF),
            jax.ShapeDtypeStruct((units, total), BF),
        ],
        compiler_params=small_vmem(),
        name="kept_half",
    )(cots, pair_own, hidden)


def sum_kernel(keep, received, out):
    out[...] = (keep[...].astype(F32) + received[...].astype(F32)).astype(BF)


def pair_sum(keep, received):
    return pl.pallas_call(
        sum_kernel,
        in_specs=in_vmem(2),
        out_specs=in_vmem(1)[0],
        out_shape=jax.ShapeDtypeStruct(keep.shape, BF),
        compiler_params=small_vmem(),
        name="pair_sum",
    )(keep, received)


def grad_kernel(core, rows_in, rows_cot, hidden_t, cots, *rest):
    gate_grad, up_grad, down_grad = rest[-3:]
    units = gate_grad.shape[1]
    both = contract(rows_in[...].T, cots[...], 1, 0).astype(BF)
    gate_grad[...] = both[:, :units]
    up_grad[...] = both[:, units:]
    down_grad[...] = contract(hidden_t[...], rows_cot[...], 1, 0).astype(BF)


def half_grads(core, flip, rows, hidden_t, cots, before=()):
    units, total = hidden_t.shape
    cols = 256
    steps = HALF // cols

    def place(i, c):
        return (1 - c[0] if flip else c[0]) * steps + i

    return pl.pallas_call(
        grad_kernel,
        grid_spec=pltpu.PrefetchScalarGridSpec(
            num_scalar_prefetch=1,
            grid=(steps,),
            in_specs=[
                pl.BlockSpec((total, cols), lambda i, c: (0, i)),
                pl.BlockSpec((total, cols), lambda i, c: (0, i + steps)),
                pl.BlockSpec((units, total), lambda i, c: (0, 0)),
                pl.BlockSpec((total, 2 * units), lambda i, c: (0, 0)),
            ]
            + [pl.BlockSpec(memory_space=pl.ANY)] * len(before),
            out_specs=[
                pl.BlockSpec((cols, units), lambda i, c: (place(i, c), 0)),
                pl.BlockSpec((cols, units), lambda i, c: (place(i, c), 0)),
                pl.BlockSpec((units, cols), lambda i, c: (0, place(i, c))),
            ],
        ),
        out_shape=[
            jax.ShapeDtypeStruct((D, units), BF),
            jax.ShapeDtypeStruct((D, units), BF),
            jax.ShapeDtypeStruct((units, D), BF),
        ],
        input_output_aliases={5 + k: k for k in range(len(before))},
        compiler_params=pltpu.CompilerParams(vmem_limit_bytes=60 * 1024 * 1024),
        name="other_grads" if flip else "own_grads",
    )(core, rows, rows, hidden_t, cots, *before)


def combine_kernel(target, rows, out):
    tokens = target.shape[0]
    row = lax.broadcasted_iota(jnp.int32, (tokens, rows.shape[0]), 1)
    hit = (row == target[:, 0:1]) | (row == target[:, 1:2])
    select = jnp.where(hit, 1.0, 0.0).astype(BF)
    width = out.shape[2]
    for pair in range(out.shape[0] // 2):
        both = jnp.dot(
            select,
            rows[:, 2 * pair * width : 2 * (pair + 1) * width],
            preferred_element_type=F32,
        ).astype(BF)
        out[2 * pair] = both[:, :width]
        out[2 * pair + 1] = both[:, width:]


def combined(target, rows):
    tokens = target.shape[0]
    cols = 128
    return pl.pallas_call(
        combine_kernel,
        in_specs=in_vmem(2),
        out_specs=in_vmem(1)[0],
        out_shape=jax.ShapeDtypeStruct((rows.shape[1] // cols, tokens, cols), BF),
        compiler_params=small_vmem(),
        name="combine",
    )(target, rows)


def mix_kernel(place, pieces, cotangent, out):
    mixed = cotangent[...].astype(F32)
    for k in range(pieces.shape[0]):
        mixed = mixed + pieces[k].astype(F32)
    for k in range(out.shape[0]):
        out[k] = mixed.astype(BF)


def mixed_copies(place, pieces, cotangent):
    depth, tokens, share = pieces.shape
    return pl.pallas_call(
        mix_kernel,
        grid_spec=pltpu.PrefetchScalarGridSpec(
            num_scalar_prefetch=1,
            grid=(1,),
            in_specs=in_vmem(1) + [pl.BlockSpec((tokens, share), lambda i, p: (0, p[0]))],
            out_specs=in_vmem(1)[0],
        ),
        out_shape=jax.ShapeDtypeStruct((depth, tokens, share), BF),
        compiler_params=small_vmem(),
        name="mix",
    )(place, pieces, cotangent)


def normalised(conv_out, mean, rstd, gain):
    centered = (conv_out[...].astype(F32) - mean[...]) * rstd[...]
    channels = conv_out.shape[0]
    column = jnp.broadcast_to(gain[...], (channels, channels)).T
    wide = jnp.concatenate([column] * (conv_out.shape[1] // channels), axis=1)
    return centered, centered * wide, wide


def norm_kernel(core, mixed_own, mixed_other, w_out, conv_out, mean, rstd, gain, norm_cot, sums):
    depth, tokens, share = mixed_own.shape
    turned = jnp.zeros((tokens, w_out.shape[1]), F32)
    for flip, mixed in ((False, mixed_own), (True, mixed_other)):
        base = (1 - core[0] if flip else core[0]) * HALF
        for k in range(depth):
            rows = pl.ds(pl.multiple_of(base + k * share, share), share)
            turned = turned + contract(mixed[k], w_out[rows, :], 1, 0)
    centered, normed, wide = normalised(conv_out, mean, rstd, gain)
    sigma = jax.nn.sigmoid(normed)
    cot = turned.T * sigma * (1.0 + normed * (1.0 - sigma)) * wide
    norm_cot[...] = cot
    first = jnp.sum(cot, axis=0, keepdims=True)
    second = jnp.sum(cot * centered, axis=0, keepdims=True)
    for k in range(sums.shape[0]):
        sums[k, 0:1, :] = first
        sums[k, 1:2, :] = second


def norm_cotangent(core, mixed_own, mixed_other, w_out, conv_out, mean, rstd, gain, copies):
    channels, tokens = conv_out.shape
    return pl.pallas_call(
        norm_kernel,
        in_specs=[SCALAR] + in_vmem(7),
        out_specs=in_vmem(2),
        out_shape=[
            jax.ShapeDtypeStruct((channels, tokens), F32),
            jax.ShapeDtypeStruct((copies, 2, tokens), F32),
        ],
        compiler_params=small_vmem(),
        name="norm_cot",
    )(core, mixed_own, mixed_other, w_out, conv_out, mean, rstd, gain)


def proj_kernel(core, mixed_own, mixed_other, conv_out, mean, rstd, gain, out):
    depth = mixed_own.shape[0]
    _, normed, _ = normalised(conv_out, mean, rstd, gain)
    act = (normed * jax.nn.sigmoid(normed)).astype(BF)
    for flip, mixed in ((False, mixed_own), (True, mixed_other)):
        base = (1 - core[0] if flip else core[0]) * depth
        for k in range(depth):
            out[base + k] = contract(act, mixed[k], 1, 0).astype(BF)


def proj_parts(core, mixed_own, mixed_other, conv_out, mean, rstd, gain):
    depth, _, share = mixed_own.shape
    return pl.pallas_call(
        proj_kernel,
        in_specs=[SCALAR] + in_vmem(6),
        out_specs=in_vmem(1)[0],
        out_shape=jax.ShapeDtypeStruct((2 * depth, conv_out.shape[0], share), BF),
        compiler_params=small_vmem(),
        name="proj_parts",
    )(core, mixed_own, mixed_other, conv_out, mean, rstd, gain)


RIM = 32


def conv_cot_kernel(sums, norm_cot, conv_out, mean, rstd, turned, rim):
    total = sums[0]
    for k in range(1, sums.shape[0]):
        total = total + sums[k]
    centered = (conv_out[...].astype(F32) - mean[...]) * rstd[...]
    cot = rstd[...] * (norm_cot[...] - total[0:1, :] / C - centered * (total[1:2, :] / C))
    across = cot.T
    turned[...] = across
    rim[...] = across[:RIM, :]


def conv_cotangent(sums, norm_cot, conv_out, mean, rstd):
    channels, tokens = conv_out.shape
    return pl.pallas_call(
        conv_cot_kernel,
        in_specs=in_vmem(5),
        out_specs=in_vmem(2),
        out_shape=[
            jax.ShapeDtypeStruct((tokens, channels), F32),
            jax.ShapeDtypeStruct((RIM, channels), F32),
        ],
        compiler_params=small_vmem(),
        name="conv_cot",
    )(sums, norm_cot, conv_out, mean, rstd)


def glu_kernel(turned, rim, taps, glu_value, glu_gate, value_grad, gate_grad, padded):
    tokens = turned.shape[0]
    padded[:tokens, :] = turned[...]
    padded[tokens:, :] = rim[...]
    total = taps[0:1, :] * turned[...]
    for lag in range(1, taps.shape[0]):
        total = total + taps[lag : lag + 1, :] * padded[lag : lag + tokens, :]
    cot = total.T
    sigma = jax.nn.sigmoid(glu_gate[...].astype(F32))
    value_grad[...] = (cot * sigma).astype(BF)
    gate_grad[...] = (cot * glu_value[...].astype(F32) * sigma * (1.0 - sigma)).astype(BF)


def glu_cotangents(turned, rim, taps, glu_value, glu_gate):
    tokens, channels = turned.shape
    return pl.pallas_call(
        glu_kernel,
        in_specs=in_vmem(5),
        out_specs=in_vmem(2),
        out_shape=[jax.ShapeDtypeStruct((channels, tokens), BF)] * 2,
        scratch_shapes=[pltpu.VMEM((tokens + RIM, channels), F32)],
        compiler_params=small_vmem(),
        name="glu_cot",
    )(turned, rim, taps, glu_value, glu_gate)


def proj_sum_kernel(parts, out):
    total = parts[0].astype(F32)
    for k in range(1, parts.shape[0]):
        total = total + parts[k].astype(F32)
    out[...] = total.T


def proj_summed(parts):
    return pl.pallas_call(
        proj_sum_kernel,
        in_specs=in_vmem(1),
        out_specs=in_vmem(1)[0],
        out_shape=jax.ShapeDtypeStruct((parts.shape[2], parts.shape[1]), F32),
        compiler_params=small_vmem(),
        name="proj_sum",
    )(parts)


def on_device(
    saved_input,
    cotangent,
    expert_ids,
    route_weight,
    w_gate,
    w_up,
    w_down,
    w_out,
    channel_gain,
    conv_taps,
    glu_value,
    glu_gate,
    conv_out,
    norm_mean,
    norm_rstd,
):
    tokens = cotangent.shape[0]
    sp_count = lax.axis_size("sp")
    experts = sp_count
    slots = 4 * tokens // experts
    tp_index = lax.axis_index("tp").astype(jnp.int32)
    core_index = tp_index & 1
    tp_count = lax.axis_size("tp")
    depth = tp_count // 2
    same_core = [[2 * z + c for z in range(depth)] for c in range(2)]
    core = core_index.reshape(1)
    place = (core_index * depth + (tp_index >> 1)).reshape(1)
    pairs = jnp.concatenate([expert_ids.astype(F32), route_weight], axis=1).T
    mine = core_index * HALF
    half_in = lax.dynamic_slice(saved_input, (0, mine), (tokens, HALF))
    half_cot = lax.dynamic_slice(cotangent, (0, mine), (tokens, HALF))
    core, place, pairs = lax.optimization_barrier((core, place, pairs))

    sent, target = routed(pairs, half_in, half_cot, experts, slots)
    own = exchanged(sent.reshape(experts, slots, D), "sp").reshape(sp_count * slots, D)
    other = swapped_cores(own)
    gate_w, up_w, down_w = w_gate[0], w_up[0], w_down[0]
    first_part, cot_part, pair_own, pair_other = own_products(core, own, gate_w, up_w, down_w)
    hidden, cots, send = other_products(core, other, first_part, cot_part, pair_other, down_w)
    received = swapped_cores(send)
    keep, hidden_t = kept_half(cots, pair_own, hidden)
    input_cot = pair_sum(keep, received)
    returned = exchanged(input_cot.reshape(sp_count, slots, HALF), "sp")

    partial = combined(target, returned.reshape(experts * slots, HALF))
    pieces = exchanged(partial, "tp", same_core)
    copies = mixed_copies(place, pieces, cotangent)
    mixed_own = exchanged(copies, "tp", same_core)
    mixed_other = swapped_cores(mixed_own)

    mixed_other, late_own, late_other, late_cots, late_hidden = lax.optimization_barrier(
        (mixed_other, own, other, cots, hidden_t)
    )
    mean, rstd = norm_mean.reshape(1, tokens), norm_rstd.reshape(1, tokens)
    gain = channel_gain.reshape(1, -1)
    norm_cot, sums = norm_cotangent(
        core, mixed_own, mixed_other, w_out, conv_out, mean, rstd, gain, tp_count
    )
    all_sums = exchanged(sums, "tp")
    proj_part = proj_parts(core, mixed_own, mixed_other, conv_out, mean, rstd, gain)
    proj_pieces = exchanged(proj_part, "sp")
    proj_grad = proj_summed(proj_pieces)
    half_done = half_grads(core, False, late_own, late_hidden, late_cots)
    all_sums, *half_done = lax.optimization_barrier((all_sums, *half_done))
    turned, rim = conv_cotangent(all_sums, norm_cot, conv_out, mean, rstd)
    rim = lax.ppermute(rim, "sp", [(i, i - 1) for i in range(1, sp_count)])
    turned, late_other = lax.optimization_barrier((turned, late_other))
    gate_grad, up_grad, down_grad = half_grads(
        core, True, late_other, late_hidden, late_cots, half_done
    )
    value_grad, gate_in_grad = glu_cotangents(turned, rim, conv_taps, glu_value, glu_gate)
    return (
        gate_grad[None],
        up_grad[None],
        down_grad[None],
        proj_grad,
        value_grad,
        gate_in_grad,
    )


def solution(mesh):
    in_specs = (
        P("sp", None),
        P("sp", None),
        P("sp", None),
        P("sp", None),
        P("sp", None, "tp"),
        P("sp", None, "tp"),
        P("sp", "tp", None),
        P(None, "tp"),
        P("tp"),
        P(None, "tp"),
        P("tp", "sp"),
        P("tp", "sp"),
        P("tp", "sp"),
        P("sp"),
        P("sp"),
    )
    out_specs = (
        P("sp", None, "tp"),
        P("sp", None, "tp"),
        P("sp", "tp", None),
        P("sp", "tp"),
        P("tp", "sp"),
        P("tp", "sp"),
    )
    return jax.shard_map(
        on_device, mesh=mesh, in_specs=in_specs, out_specs=out_specs, check_vma=False
    )
```

time: 377 us -> 195 us (0.52); the launches traced: 370 us -> 194 us
  waiting for transfers between devices: 95.9 us -> 13.6 us
  local copies, waits for them, and re-layouts: 64.6 us -> 2.22 us
  matrix products: 34.5 us -> 0 us
  Pallas kernels: 0 us -> 30.8 us
  other arithmetic: 29.5 us -> 1.37 us
  blocking collectives: 114 us -> 130 us
  between operations: 14.9 us -> 0.88 us
    reduce_scatter x1 -> x0, waiting for transfers between devices: 64.5 us -> none  [on_device(): lax.psum_scatter(blocks.astype(jnp.bfloat16), 'tp', scatter_dimension=2,...]
    dot_general x10 -> x0, matrix products: 34.5 us -> none  [the longest x8 29.9 us: contract(): lax.dot_general(left, right, (((left_dim,), (right_dim,)), ((), ())), pre...]
    pallas_call x0 -> x14, Pallas kernels: none -> 30.8 us  [the longest x2 13.4 us: half_grads(): pl.pallas_call(grad_kernel, grid_spec=pltpu.PrefetchScalarGridSpec(num_sc...]
    all_gather x1 -> x0, waiting for transfers between devices: 26.8 us -> none  [on_device(): lax.all_gather(returned.astype(jnp.bfloat16), 'tp', axis=2, tiled=True)]
    gather x3 -> x0, local copies, waits for them, and re-layouts: 25.6 us -> none  [the longest x1 10.8 us: on_device(): scaled[pair_index]]
    all_to_all x2 -> x4, blocking collectives: 114 us -> 130 us  [exchanged(): lax.all_to_all(value, axis, 0, 0, axis_index_groups=groups, tiled=True)]
    reshape x2 -> x0, local copies, waits for them, and re-layouts: 13.9 us -> none  [on_device(): whole.reshape(expert_count * capacity, D)[target].reshape(tokens_here, 2, D)]
    mul x7 -> x0, local copies, waits for them, and re-layouts: 11.9 us -> none  [the longest x3 11.6 us: on_device(): route_weight[:, :, None] * cotangent.astype(jnp.float32)[:, None, :]]
  transfers between devices with their start and end apart: 5 -> 6, of which waited for: 3 -> 4; matrix products, arithmetic and copies ran while one was open for 6% -> 0% of each run, Pallas kernels for 0% -> 11%
where the time goes in v1:
time: 195 us; the launch traced here: 194 us
  blocking collectives  130 us (67%)
  Pallas kernels  30.8 us (16%)
  starting transfers between devices  15.2 us (8%)
  waiting for transfers between devices  13.6 us (7%)
  local copies, waits for them, and re-layouts  2.22 us (1%)
    all_to_all x4, blocking collectives, exchanged(): lax.all_to_all(value, axis, 0, 0, axis_index_groups=groups, tiled=True)  130 us
    pallas_call x2, Pallas kernels, half_grads(): pl.pallas_call(grad_kernel, grid_spec=pltpu.PrefetchScalarGridSpec(num_sc...  13.4 us
    all_to_all x2, starting transfers between devices, exchanged(): lax.all_to_all(value, axis, 0, 0, axis_index_groups=groups, tiled=True)  9.96 us
    ppermute x3, waiting for transfers between devices, swapped_cores(): return lax.ppermute(value, 'tp', pairs)  7.23 us
    all_to_all x2, waiting for transfers between devices, exchanged(): lax.all_to_all(value, axis, 0, 0, axis_index_groups=groups, tiled=True)  6.37 us
    pallas_call x1, Pallas kernels, other_products(): pl.pallas_call(other_kernel, in_specs=[SCALAR] + in_vmem(5), out_specs=in...  5.12 us
    ppermute x1, starting transfers between devices, on_device(): rim = lax.ppermute(rim, 'sp', [(i, i - 1) for i in range(1, sp_count)])  4.88 us
  transfers between devices with their start and end apart: 6, of which 4 were waited for; matrix products, arithmetic and copies ran while one was open for 0% of the time, Pallas kernels for 11%

profile of v1, /device:TPU:24, one launch (start us, length us, event | category | flops | bytes accessed | tf_op | source)
XLA Modules:
  0.0 194.3 jit_solution(15499937655259837189)
XLA Ops:
  0.6 0.7 convert_element_type.3
  1.3 0.7 maximum_bitcast_fusion.pairs
  2.0 1.3 constant_dynamic-slice_fusion
  3.3 1.6 route.1
  4.9 0.0 copy-start.3
  4.9 0.0 copy-start.6
  4.9 0.0 copy-start.7
  4.9 55.8 %all_to_all.30 = bf16[16,64,2048]{2,1,0:T(8,128)(2,1)S(1)} all-to-all(bf16[16,64,2048]{2,1,0:T(8,128)(2,1)S(1)} %bitcast.25), channel_id=1, replica_groups=mesh['sp'=16,'tp'=16] {'sp'}, dimensions={0} | all-to-all | bytes 8388608 | tf_op jit(solution)/shard_map/all_to_all | solution.py:25
  60.7 0.0 collective-permute-start
  60.8 3.0 %own_products.1 = (f32[1024,768]{1,0:T(8,128)S(1)}, f32[1024,384]{1,0:T(8,128)S(1)}, bf16[1024,768]{1,0:T(8,128)(2,1)S(1)}, bf16[1024,768]{1,0:T(8,128)(2,1)S(1)}) custom-call(s32[1]{0:T(128)} %bitcast.core, bf16[1024,2048]{1,0:T(8,128)(2,1)S(1)} %bitcast.18, bf16[2048,384]{1,0:T(8,128)(2,1)S(1)} %bitcast.26, bf16[2048,384]{1,0:T(8,128)(2,1)S(1)} %bitcast.27, ...), custom_call_target="tpu_custom_call" | custom-call | tf_op jit(solution)/shard_map/own_products/pallas_call | solution.py:119
  63.8 4.1 %collective-permute-done.other.rows_in.rows_cot = bf16[1024,2048]{1,0:T(8,128)(2,1)S(1)} collective-permute-done((bf16[1024,2048]{1,0:T(8,128)(2,1)S(1)}, bf16[1024,2048]{1,0:T(8,128)(2,1)S(1)}, u32[]{:S(2)}, u32[]{:S(2)}) %collective-permute-start) | collective-permute-done | bytes 4194336 | tf_op jit(solution)/shard_map/ppermute | solution.py:30
  67.9 5.1 %other_products.1 = (bf16[1024,384]{1,0:T(8,128)(2,1)S(1)}, bf16[1024,768]{1,0:T(8,128)(2,1)S(1)}, bf16[1024,1024]{1,0:T(8,128)(2,1)S(1)}) custom-call(s32[1]{0:T(128)} %bitcast.core, bf16[1024,2048]{1,0:T(8,128)(2,1)S(1)} %collective-permute-done.other.rows_in.rows_cot, f32[1024,768]{1,0:T(8,128)S(1)} %get-tuple-element.48.first_part, ...), custom_call_target="tpu_custom_call" | custom-call | tf_op jit(solution)/shard_map/other_products/pallas_call | solution.py:156
  73.0 0.0 copy-done.1
  73.0 0.0 copy-start.2
  73.1 0.4 collective-permute-start.1
  73.5 1.9 kept_half.1
  75.3 0.0 copy-done.2
  75.3 0.0 copy-start.4
  75.3 0.9 copy-done.4
  76.2 1.3 collective-permute-done.1.received
  77.5 0.5 pair_sum.1
  78.0 31.6 %all_to_all.31 = bf16[16,64,1024]{2,1,0:T(8,128)(2,1)S(1)} all-to-all(bf16[16,64,1024]{2,1,0:T(8,128)(2,1)S(1)} %bitcast.21), channel_id=1, replica_groups=mesh['sp'=16,'tp'=16] {'sp'}, dimensions={0} | all-to-all | bytes 4194304 | tf_op jit(solution)/shard_map/all_to_all | solution.py:25
  109.6 0.8 combine.1
  110.4 24.7 %all_to_all.32.pieces = bf16[8,256,128]{2,1,0:T(8,128)(2,1)S(1)} all-to-all(bf16[8,256,128]{2,1,0:T(8,128)(2,1)S(1)} %combine.1), channel_id=1, replica_groups={{0,2,4,6,8,10,12,14},{1,3,5,7,9,11,13,15},{16,18,20,22,24,26,28,30},{17..., dimensions={0} | all-to-all | bytes 1048576 | tf_op jit(solution)/shard_map/all_to_all | solution.py:25
  135.1 0.0 copy-start.14
  135.1 0.0 copy-start.15
  135.1 0.2 mix.1
  135.3 18.1 %all_to_all.33.mixed_own = bf16[8,256,128]{2,1,0:T(8,128)(2,1)S(1)} all-to-all(bf16[8,256,128]{2,1,0:T(8,128)(2,1)S(1)} %mix.1), channel_id=1, replica_groups={{0,2,4,6,8,10,12,14},{1,3,5,7,9,11,13,15},{16,18,20,22,24,26,28,30},{17..., dimensions={0} | all-to-all | bytes 1048576 | tf_op jit(solution)/shard_map/all_to_all | solution.py:25
  153.4 0.0 collective-permute-start.2
  153.4 1.9 collective-permute-done.2.mixed_other
  155.3 0.0 copy-done.14
  155.3 0.0 copy-done.15
  155.3 1.1 norm_cot.1
  156.4 3.5 %all-to-all-start.4 = ((f32[16,2,256]{2,1,0:T(2,128)}), f32[16,2,256]{2,1,0:T(2,128)S(1)}, u32[]{:S(2)}, u32[]{:S(2)}) async-start(f32[16,2,256]{2,1,0:T(2,128)} %get-tuple-element.58), calls=%async_computation.4 | async-start | bytes 65536 | tf_op jit(solution)/shard_map/all_to_all | solution.py:25
  160.0 1.3 proj_parts.1
  161.2 6.4 %all-to-all-done.4.sums = f32[16,2,256]{2,1,0:T(2,128)S(1)} async-done(((f32[16,2,256]{2,1,0:T(2,128)}), f32[16,2,256]{2,1,0:T(2,128)S(1)}, u32[]{:S(2)}, u32[]{:S(2)}) %all-to-all-start.4) | async-done | bytes 32800 | tf_op jit(solution)/shard_map/all_to_all | solution.py:25
  167.6 6.5 %all-to-all-start.5 = ((bf16[16,128,128]{2,1,0:T(8,128)(2,1)}), bf16[16,128,128]{2,1,0:T(8,128)(2,1)S(1)}, u32[]{:S(2)}, u32[]{:S(2)}) async-start(bf16[16,128,128]{2,1,0:T(8,128)(2,1)} %proj_parts.1), calls=%async_computation.5 | async-start | bytes 1048576 | tf_op jit(solution)/shard_map/all_to_all | solution.py:25
  174.1 6.7 %own_grads.1 = (bf16[2048,384]{1,0:T(8,128)(2,1)}, bf16[2048,384]{1,0:T(8,128)(2,1)}, bf16[384,2048]{1,0:T(8,128)(2,1)}) custom-call(s32[1]{0:T(128)} %bitcast.core, bf16[1024,2048]{1,0:T(8,128)(2,1)} %bitcast.19, bf16[1024,2048]{1,0:T(8,128)(2,1)} %bitcast.20, bf16[384,1024]{1,0:T(8,128)(2,1)} %copy-done.4, bf16[1024,768]{1,0:T(8,128)(2,1)} %copy-done.2), custom_call_target="tpu_custom_call" | custom-call | tf_op jit(solution)/shard_map/own_grads/pallas_call | solution.py:224
  180.8 0.1 conv_cot.1
  180.9 4.9 %collective-permute-start.3 = (f32[32,128]{1,0:T(8,128)S(1)}, f32[32,128]{1,0:T(8,128)S(1)}, u32[]{:S(2)}, u32[]{:S(2)}) collective-permute-start(f32[32,128]{1,0:T(8,128)S(1)} %get-tuple-element.77), channel_id=1, source_target_pairs={{16,0},{32,16},{48,32},{64,48},{80,64},{96,80},{112,96},{128,112},... | collective-permute-start | bytes 49160 | tf_op jit(solution)/shard_map/ppermute | solution.py:509
  185.8 0.0 copy-start.10
  185.8 0.0 copy-start.11
  185.8 0.0 copy-start.12
  185.8 6.7 %other_grads.1 = (bf16[2048,384]{1,0:T(8,128)(2,1)}, bf16[2048,384]{1,0:T(8,128)(2,1)}, bf16[384,2048]{1,0:T(8,128)(2,1)}) custom-call(s32[1]{0:T(128)} %bitcast.core, bf16[1024,2048]{1,0:T(8,128)(2,1)} %copy-done.1, bf16[1024,2048]{1,0:T(8,128)(2,1)} %copy-done.1, ...), custom_call_target="tpu_custom_call", output_to_operand_aliasing={{0}: (5, {}), {1}: (6, {}), {2}: (7, {})} | custom-call | tf_op jit(solution)/shard_map/other_grads/pallas_call | solution.py:224
  192.5 0.0 collective-permute-done.3.rim
  192.5 1.0 glu_cot.1
  193.6 0.0 all-to-all-done.5.parts
  193.6 0.8 proj_sum.1
  (17 shorter events, 0.0 us)
Async XLA Ops:
  4.9 55.8 %copy-start.3 = (bf16[1,384,2048]{2,1,0:T(8,128)(2,1)S(1)}, bf16[1,384,2048]{2,1,0:T(8,128)(2,1)}, u32[]{:S(2)}) copy-start(bf16[1,384,2048]{2,1,0:T(8,128)(2,1)} %param.21) | copy-start | bytes 4718596
  4.9 55.8 %copy-start.6 = (bf16[1,2048,384]{2,1,0:T(8,128)(2,1)S(1)}, bf16[1,2048,384]{2,1,0:T(8,128)(2,1)}, u32[]{:S(2)}) copy-start(bf16[1,2048,384]{2,1,0:T(8,128)(2,1)} %param.19) | copy-start | bytes 4718596
  4.9 55.8 %copy-start.7 = (bf16[1,2048,384]{2,1,0:T(8,128)(2,1)S(1)}, bf16[1,2048,384]{2,1,0:T(8,128)(2,1)}, u32[]{:S(2)}) copy-start(bf16[1,2048,384]{2,1,0:T(8,128)(2,1)} %param.20) | copy-start | bytes 4718596
  60.7 3.1 %copy-start = (bf16[16,64,2048]{2,1,0:T(8,128)(2,1)}, bf16[16,64,2048]{2,1,0:T(8,128)(2,1)S(1)}, u32[]{:S(2)}) copy-start(bf16[16,64,2048]{2,1,0:T(8,128)(2,1)S(1)} %all_to_all.30) | copy-start | bytes 12582916
  60.7 7.2 %collective-permute-start = (bf16[1024,2048]{1,0:T(8,128)(2,1)S(1)}, bf16[1024,2048]{1,0:T(8,128)(2,1)S(1)}, u32[]{:S(2)}, u32[]{:S(2)}) collective-permute-start(bf16[1024,2048]{1,0:T(8,128)(2,1)S(1)} %bitcast.17), channel_id=1, source_target_pairs={{0,1},{1,0},{2,3},{3,2},{4,5},{5,4},{6,7},{7,6},{8,9},{9,8},{10,11... | collective-permute-start | bytes 12582920 | tf_op jit(solution)/shard_map/ppermute | solution.py:30
  67.9 5.1 %copy-start.1 = (bf16[1024,2048]{1,0:T(8,128)(2,1)}, bf16[1024,2048]{1,0:T(8,128)(2,1)S(1)}, u32[]{:S(2)}) copy-start(bf16[1024,2048]{1,0:T(8,128)(2,1)S(1)} %collective-permute-done.other.rows_in.rows_cot) | copy-start | bytes 12582916
  73.0 2.3 %copy-start.2 = (bf16[1024,768]{1,0:T(8,128)(2,1)}, bf16[1024,768]{1,0:T(8,128)(2,1)S(1)}, u32[]{:S(2)}) copy-start(bf16[1024,768]{1,0:T(8,128)(2,1)S(1)} %get-tuple-element.61.cots) | copy-start | bytes 4718596
  73.1 4.4 %collective-permute-start.1 = (bf16[1024,1024]{1,0:T(8,128)(2,1)S(1)}, bf16[1024,1024]{1,0:T(8,128)(2,1)S(1)}, u32[]{:S(2)}, u32[]{:S(2)}) collective-permute-start(bf16[1024,1024]{1,0:T(8,128)(2,1)S(1)} %get-tuple-element.55), channel_id=1, source_target_pairs={{0,1},{1,0},{2,3},{3,2},{4,5},{5,4},{6,7},{7,6},{8,9},{9,8},{10,11... | collective-permute-start | bytes 6291464 | tf_op jit(solution)/shard_map/ppermute | solution.py:30
  75.3 0.9 copy-start.4
  109.6 25.5 %copy-start.5 = (bf16[256,2048]{1,0:T(8,128)(2,1)S(1)}, bf16[256,2048]{1,0:T(8,128)(2,1)}, u32[]{:S(2)}) copy-start(bf16[256,2048]{1,0:T(8,128)(2,1)} %cotangent.1) | copy-start | bytes 3145732
  135.1 20.2 %copy-start.8 = (bf16[128,256]{1,0:T(8,128)(2,1)S(1)}, bf16[128,256]{1,0:T(8,128)(2,1)}, u32[]{:S(2)}) copy-start(bf16[128,256]{1,0:T(8,128)(2,1)} %conv_out.5) | copy-start | bytes 196612
  135.1 20.2 %copy-start.9 = (bf16[2048,128]{1,0:T(8,128)(2,1)S(1)}, bf16[2048,128]{1,0:T(8,128)(2,1)}, u32[]{:S(2)}) copy-start(bf16[2048,128]{1,0:T(8,128)(2,1)} %w_out.1) | copy-start | bytes 1572868
  135.1 20.2 %copy-start.13 = (f32[256]{0:T(256)S(1)}, f32[256]{0:T(256)}, u32[]{:S(2)}) copy-start(f32[256]{0:T(256)} %param.28) | copy-start | bytes 3076
  135.1 20.2 %copy-start.14 = (f32[256]{0:T(256)S(1)}, f32[256]{0:T(256)}, u32[]{:S(2)}) copy-start(f32[256]{0:T(256)} %param.29) | copy-start | bytes 3076
  135.1 20.2 %copy-start.15 = (f32[128]{0:T(128)S(1)}, f32[128]{0:T(128)}, u32[]{:S(2)}) copy-start(f32[128]{0:T(128)} %param.23) | copy-start | bytes 1540
  153.4 1.9 collective-permute-start.2
  156.4 11.2 %all-to-all-start.4 = ((f32[16,2,256]{2,1,0:T(2,128)}), f32[16,2,256]{2,1,0:T(2,128)S(1)}, u32[]{:S(2)}, u32[]{:S(2)}) async-start(f32[16,2,256]{2,1,0:T(2,128)} %get-tuple-element.58), calls=%async_computation.4 | async-start | bytes 65536 | tf_op jit(solution)/shard_map/all_to_all | solution.py:25
  167.6 26.0 %all-to-all-start.5 = ((bf16[16,128,128]{2,1,0:T(8,128)(2,1)}), bf16[16,128,128]{2,1,0:T(8,128)(2,1)S(1)}, u32[]{:S(2)}, u32[]{:S(2)}) async-start(bf16[16,128,128]{2,1,0:T(8,128)(2,1)} %proj_parts.1), calls=%async_computation.5 | async-start | bytes 1048576 | tf_op jit(solution)/shard_map/all_to_all | solution.py:25
  180.9 11.6 %collective-permute-start.3 = (f32[32,128]{1,0:T(8,128)S(1)}, f32[32,128]{1,0:T(8,128)S(1)}, u32[]{:S(2)}, u32[]{:S(2)}) collective-permute-start(f32[32,128]{1,0:T(8,128)S(1)} %get-tuple-element.77), channel_id=1, source_target_pairs={{16,0},{32,16},{48,32},{64,48},{80,64},{96,80},{112,96},{128,112},... | collective-permute-start | bytes 49160 | tf_op jit(solution)/shard_map/ppermute | solution.py:509
  185.8 6.7 %copy-start.10 = (bf16[128,256]{1,0:T(8,128)(2,1)S(1)}, bf16[128,256]{1,0:T(8,128)(2,1)}, u32[]{:S(2)}) copy-start(bf16[128,256]{1,0:T(8,128)(2,1)} %glu_value.1) | copy-start | bytes 196612
  185.8 6.7 %copy-start.11 = (bf16[128,256]{1,0:T(8,128)(2,1)S(1)}, bf16[128,256]{1,0:T(8,128)(2,1)}, u32[]{:S(2)}) copy-start(bf16[128,256]{1,0:T(8,128)(2,1)} %glu_gate.1) | copy-start | bytes 196612
  185.8 6.7 %copy-start.12 = (f32[31,128]{1,0:T(8,128)S(1)}, f32[31,128]{1,0:T(8,128)}, u32[]{:S(2)}) copy-start(f32[31,128]{1,0:T(8,128)} %taps.1) | copy-start | bytes 47620

commit v2 on v1

--- a/solution.py
+++ b/solution.py
@@ -101,7 +101,10 @@
     return pl.ds(pl.multiple_of(index * HALF, HALF), HALF)
 
 
-def own_kernel(core, own, w_gate, w_up, w_down, first_part, cot_part, pair_own, pair_other):
+def own_kernel(
+    core, own, w_gate, w_up, w_down, first_part, cot_part, own_t, pair_other, other_t, down_t,
+    pair_own,
+):
     units = w_gate.shape[1]
     half, far = half_of(core, False), half_of(core, True)
     pair_own[:, :units] = w_gate[half, :]
@@ -112,6 +115,9 @@
         cot_part[here, :] = contract(own[here, HALF:], w_down[:, half], 1, 1)
     pair_other[:, :units] = w_gate[far, :]
     pair_other[:, units:] = w_up[far, :]
+    down_t[...] = w_down[:, far].T
+    other_t[...] = pair_other[...].T
+    own_t[...] = pair_own[...].T
 
 
 def own_products(core, own, w_gate, w_up, w_down):
@@ -119,43 +125,45 @@
     return pl.pallas_call(
         own_kernel,
         in_specs=[SCALAR] + in_vmem(4),
-        out_specs=in_vmem(4),
+        out_specs=in_vmem(6),
         out_shape=[
             jax.ShapeDtypeStruct((total, 2 * units), F32),
             jax.ShapeDtypeStruct((total, units), F32),
+            jax.ShapeDtypeStruct((2 * units, HALF), BF),
             jax.ShapeDtypeStruct((HALF, 2 * units), BF),
-            jax.ShapeDtypeStruct((HALF, 2 * units), BF),
-        ],
+            jax.ShapeDtypeStruct((2 * units, HALF), BF),
+            jax.ShapeDtypeStruct((HALF, units), BF),
+        ],
+        scratch_shapes=[pltpu.VMEM((HALF, 2 * units), BF)],
         compiler_params=small_vmem(),
         name="own_products",
     )(core, own, w_gate, w_up, w_down)
 
 
 def other_kernel(
-    core, other, first_part, cot_part, pair_other, w_down, hidden_out, cots, send,
+    other, first_part, cot_part, pair_other, other_t, down_t, hidden, cots, send,
 ):
-    half = half_of(core, True)
-    units = w_down.shape[0]
+    units = down_t.shape[1]
     for step in range(other.shape[0] // ROWS):
         here = slice(step * ROWS, (step + 1) * ROWS)
         first = first_part[here, :] + contract(other[here, :HALF], pair_other[...], 1, 0)
         gate_pre, up_pre = first[:, :units], first[:, units:]
-        hidden_cot = cot_part[here, :] + contract(other[here, HALF:], w_down[:, half], 1, 1)
+        hidden_cot = cot_part[here, :] + contract(other[here, HALF:], down_t[...], 1, 0)
         sigma = jax.nn.sigmoid(gate_pre)
         silu = gate_pre * sigma
-        hidden_out[here, :] = (silu * up_pre).astype(BF)
+        hidden[here, :] = (silu * up_pre).astype(BF)
         cots[here, :units] = (
             hidden_cot * up_pre * sigma * (1.0 + gate_pre * (1.0 - sigma))
         ).astype(BF)
         cots[here, units:] = (hidden_cot * silu).astype(BF)
-        send[here, :] = contract(cots[here, :], pair_other[...], 1, 1).astype(BF)
-
-
-def other_products(core, other, first_part, cot_part, pair_other, w_down):
-    total, units = other.shape[0], w_down.shape[0]
+        send[here, :] = contract(cots[here, :], other_t[...], 1, 0).astype(BF)
+
+
+def other_products(other, first_part, cot_part, pair_other, other_t, down_t):
+    total, units = other.shape[0], down_t.shape[1]
     return pl.pallas_call(
         other_kernel,
-        in_specs=[SCALAR] + in_vmem(5),
+        in_specs=in_vmem(6),
         out_specs=in_vmem(3),
         out_shape=[
             jax.ShapeDtypeStruct((total, units), BF),
@@ -164,17 +172,17 @@
         ],
         compiler_params=small_vmem(),
         name="other_products",
-    )(core, other, first_part, cot_part, pair_other, w_down)
-
-
-def keep_kernel(cots, pair_own, hidden, keep, hidden_t):
+    )(other, first_part, cot_part, pair_other, other_t, down_t)
+
+
+def keep_kernel(cots, own_t, hidden, keep, hidden_t):
     for step in range(keep.shape[0] // ROWS):
         here = slice(step * ROWS, (step + 1) * ROWS)
-        keep[here, :] = contract(cots[here, :], pair_own[...], 1, 1).astype(BF)
+        keep[here, :] = contract(cots[here, :], own_t[...], 1, 0).astype(BF)
     hidden_t[...] = hidden[...].T
 
 
-def kept_half(cots, pair_own, hidden):
+def kept_half(cots, own_t, hidden):
     total, units = hidden.shape
     return pl.pallas_call(
         keep_kernel,
@@ -186,7 +194,7 @@
         ],
         compiler_params=small_vmem(),
         name="kept_half",
-    )(cots, pair_own, hidden)
+    )(cots, own_t, hidden)
 
 
 def sum_kernel(keep, received, out):
@@ -311,26 +319,53 @@
     return centered, centered * wide, wide
 
 
-def norm_kernel(core, mixed_own, mixed_other, w_out, conv_out, mean, rstd, gain, norm_cot, sums):
-    depth, tokens, share = mixed_own.shape
-    turned = jnp.zeros((tokens, w_out.shape[1]), F32)
-    for flip, mixed in ((False, mixed_own), (True, mixed_other)):
-        base = (1 - core[0] if flip else core[0]) * HALF
-        for k in range(depth):
-            rows = pl.ds(pl.multiple_of(base + k * share, share), share)
-            turned = turned + contract(mixed[k], w_out[rows, :], 1, 0)
+def mixed_kernel(core, mixed, w_out, conv_out, mean, rstd, gain, turned, parts):
+    depth, tokens, share = mixed.shape
+    _, normed, _ = normalised(conv_out, mean, rstd, gain)
+    act = (normed * jax.nn.sigmoid(normed)).astype(BF)
+    total = jnp.zeros((tokens, w_out.shape[1]), F32)
+    for k in range(depth):
+        rows = pl.ds(pl.multiple_of(core[0] * HALF + k * share, share), share)
+        total = total + contract(mixed[k], w_out[rows, :], 1, 0)
+        parts[k] = contract(act, mixed[k], 1, 0).astype(BF)
+    turned[...] = total
+
+
+def own_mixed_products(core, mixed, w_out, conv_out, mean, rstd, gain):
+    depth, tokens, share = mixed.shape
+    channels = w_out.shape[1]
+    return pl.pallas_call(
+        mixed_kernel,
+        in_specs=[SCALAR] + in_vmem(6),
+        out_specs=in_vmem(2),
+        out_shape=[
+            jax.ShapeDtypeStruct((tokens, channels), F32),
+            jax.ShapeDtypeStruct((depth, channels, share), BF),
+        ],
+        compiler_params=small_vmem(),
+        name="own_mixed",
+    )(core, mixed, w_out, conv_out, mean, rstd, gain)
+
+
+def norm_kernel(core, mixed, turned_part, w_out, conv_out, mean, rstd, gain, norm_cot, sums):
+    depth, _, share = mixed.shape
+    turned = turned_part[...]
+    base = (1 - core[0]) * HALF
+    for k in range(depth):
+        rows = pl.ds(pl.multiple_of(base + k * share, share), share)
+        turned = turned + contract(mixed[k], w_out[rows, :], 1, 0)
     centered, normed, wide = normalised(conv_out, mean, rstd, gain)
     sigma = jax.nn.sigmoid(normed)
     cot = turned.T * sigma * (1.0 + normed * (1.0 - sigma)) * wide
     norm_cot[...] = cot
     first = jnp.sum(cot, axis=0, keepdims=True)
     second = jnp.sum(cot * centered, axis=0, keepdims=True)
+    both = jnp.concatenate([first, second], axis=0)
     for k in range(sums.shape[0]):
-        sums[k, 0:1, :] = first
-        sums[k, 1:2, :] = second
-
-
-def norm_cotangent(core, mixed_own, mixed_other, w_out, conv_out, mean, rstd, gain, copies):
+        sums[k] = both
+
+
+def norm_cotangent(core, mixed, turned_part, w_out, conv_out, mean, rstd, gain, copies):
     channels, tokens = conv_out.shape
     return pl.pallas_call(
         norm_kernel,
@@ -342,29 +377,28 @@
         ],
         compiler_params=small_vmem(),
         name="norm_cot",
-    )(core, mixed_own, mixed_other, w_out, conv_out, mean, rstd, gain)
-
-
-def proj_kernel(core, mixed_own, mixed_other, conv_out, mean, rstd, gain, out):
-    depth = mixed_own.shape[0]
+    )(core, mixed, turned_part, w_out, conv_out, mean, rstd, gain)
+
+
+def proj_kernel(core, mixed, own_parts, conv_out, mean, rstd, gain, out):
+    depth = mixed.shape[0]
     _, normed, _ = normalised(conv_out, mean, rstd, gain)
     act = (normed * jax.nn.sigmoid(normed)).astype(BF)
-    for flip, mixed in ((False, mixed_own), (True, mixed_other)):
-        base = (1 - core[0] if flip else core[0]) * depth
-        for k in range(depth):
-            out[base + k] = contract(act, mixed[k], 1, 0).astype(BF)
-
-
-def proj_parts(core, mixed_own, mixed_other, conv_out, mean, rstd, gain):
-    depth, _, share = mixed_own.shape
+    for k in range(depth):
+        out[core[0] * depth + k] = own_parts[k]
+        out[(1 - core[0]) * depth + k] = contract(act, mixed[k], 1, 0).astype(BF)
+
+
+def proj_parts(core, mixed, own_parts, conv_out, mean, rstd, gain):
+    depth, channels, share = own_parts.shape
     return pl.pallas_call(
         proj_kernel,
         in_specs=[SCALAR] + in_vmem(6),
         out_specs=in_vmem(1)[0],
-        out_shape=jax.ShapeDtypeStruct((2 * depth, conv_out.shape[0], share), BF),
+        out_shape=jax.ShapeDtypeStruct((2 * depth, channels, share), BF),
         compiler_params=small_vmem(),
         name="proj_parts",
-    )(core, mixed_own, mixed_other, conv_out, mean, rstd, gain)
+    )(core, mixed, own_parts, conv_out, mean, rstd, gain)
 
 
 RIM = 32
@@ -478,10 +512,12 @@
     own = exchanged(sent.reshape(experts, slots, D), "sp").reshape(sp_count * slots, D)
     other = swapped_cores(own)
     gate_w, up_w, down_w = w_gate[0], w_up[0], w_down[0]
-    first_part, cot_part, pair_own, pair_other = own_products(core, own, gate_w, up_w, down_w)
-    hidden, cots, send = other_products(core, other, first_part, cot_part, pair_other, down_w)
+    first_part, cot_part, own_t, pair_other, other_t, down_t = own_products(
+        core, own, gate_w, up_w, down_w
+    )
+    hidden, cots, send = other_products(other, first_part, cot_part, pair_other, other_t, down_t)
     received = swapped_cores(send)
-    keep, hidden_t = kept_half(cots, pair_own, hidden)
+    keep, hidden_t = kept_half(cots, own_t, hidden)
     input_cot = pair_sum(keep, received)
     returned = exchanged(input_cot.reshape(sp_count, slots, HALF), "sp")
 
@@ -490,19 +526,21 @@
     copies = mixed_copies(place, pieces, cotangent)
     mixed_own = exchanged(copies, "tp", same_core)
     mixed_other = swapped_cores(mixed_own)
-
+    mean, rstd = norm_mean.reshape(1, tokens), norm_rstd.reshape(1, tokens)
+    gain = channel_gain.reshape(1, -1)
+    turned_part, own_parts = own_mixed_products(
+        core, mixed_own, w_out, conv_out, mean, rstd, gain
+    )
+    norm_cot, sums = norm_cotangent(
+        core, mixed_other, turned_part, w_out, conv_out, mean, rstd, gain, tp_count
+    )
+    all_sums = exchanged(sums, "tp")
+    proj_part = proj_parts(core, mixed_other, own_parts, conv_out, mean, rstd, gain)
+    proj_pieces = exchanged(proj_part, "sp")
+    proj_grad = proj_summed(proj_pieces)
     mixed_other, late_own, late_other, late_cots, late_hidden = lax.optimization_barrier(
         (mixed_other, own, other, cots, hidden_t)
     )
-    mean, rstd = norm_mean.reshape(1, tokens), norm_rstd.reshape(1, tokens)
-    gain = channel_gain.reshape(1, -1)
-    norm_cot, sums = norm_cotangent(
-        core, mixed_own, mixed_other, w_out, conv_out, mean, rstd, gain, tp_count
-    )
-    all_sums = exchanged(sums, "tp")
-    proj_part = proj_parts(core, mixed_own, mixed_other, conv_out, mean, rstd, gain)
-    proj_pieces = exchanged(proj_part, "sp")
-    proj_grad = proj_summed(proj_pieces)
     half_done = half_grads(core, False, late_own, late_hidden, late_cots)
     all_sums, *half_done = lax.optimization_barrier((all_sums, *half_done))
     turned, rim = conv_cotangent(all_sums, norm_cot, conv_out, mean, rstd)

time: 195 us -> 195 us (level)
    pallas_call x1 -> x2, Pallas kernels: 5.12 us -> 5.66 us  [the longest x1 5.18 us: other_products(): pl.pallas_call(other_kernel, in_specs=in_vmem(6), out_specs=in_vmem(3), o...]
where the time goes in v2:
time: 195 us; the launch traced here: 194 us
  blocking collectives  130 us (67%)
  Pallas kernels  31.1 us (16%)
  starting transfers between devices  15.2 us (8%)
  waiting for transfers between devices  13.2 us (7%)
  local copies, waits for them, and re-layouts  2.22 us (1%)
    all_to_all x4, blocking collectives, exchanged(): lax.all_to_all(value, axis, 0, 0, axis_index_groups=groups, tiled=True)  130 us
    pallas_call x2, Pallas kernels, half_grads(): pl.pallas_call(grad_kernel, grid_spec=pltpu.PrefetchScalarGridSpec(num_sc...  13.4 us
    all_to_all x2, starting transfers between devices, exchanged(): lax.all_to_all(value, axis, 0, 0, axis_index_groups=groups, tiled=True)  9.95 us
    ppermute x3, waiting for transfers between devices, swapped_cores(): return lax.ppermute(value, 'tp', pairs)  6.65 us
    all_to_all x2, waiting for transfers between devices, exchanged(): lax.all_to_all(value, axis, 0, 0, axis_index_groups=groups, tiled=True)  6.51 us
    pallas_call x1, Pallas kernels, other_products(): pl.pallas_call(other_kernel, in_specs=in_vmem(6), out_specs=in_vmem(3), o...  5.18 us
    ppermute x1, starting transfers between devices, on_device(): rim = lax.ppermute(rim, 'sp', [(i, i - 1) for i in range(1, sp_count)])  4.87 us
  transfers between devices with their start and end apart: 6, of which 4 were waited for; matrix products, arithmetic and copies ran while one was open for 0% of the time, Pallas kernels for 11%

profile of v2, /device:TPU:24, one launch (start us, length us, event | category | flops | bytes accessed | tf_op | source)
XLA Modules:
  0.0 194.2 jit_solution(15928640799936180794)
XLA Ops:
  0.6 0.7 convert_element_type.3
  1.3 0.7 maximum_bitcast_fusion.pairs
  2.0 1.3 constant_dynamic-slice_fusion
  3.3 1.6 route.1
  4.9 0.0 copy-start.6
  4.9 0.0 copy-start.7
  4.9 0.0 copy-start.8
  4.9 55.8 %all_to_all.30 = bf16[16,64,2048]{2,1,0:T(8,128)(2,1)S(1)} all-to-all(bf16[16,64,2048]{2,1,0:T(8,128)(2,1)S(1)} %bitcast.23), channel_id=1, replica_groups=mesh['sp'=16,'tp'=16] {'sp'}, dimensions={0} | all-to-all | bytes 8388608 | tf_op jit(solution)/shard_map/all_to_all | solution.py:25
  60.7 0.0 collective-permute-start
  60.8 0.0 copy-done.6
  60.8 3.2 %own_products.1 = (f32[1024,768]{1,0:T(8,128)S(1)}, f32[1024,384]{1,0:T(8,128)S(1)}, bf16[768,1024]{1,0:T(8,128)(2,1)S(1)}, bf16[1024,768]{1,0:T(8,128)(2,1)S(1)...) custom-call(s32[1]{0:T(128)} %bitcast.core, bf16[1024,2048]{1,0:T(8,128)(2,1)S(1)} %bitcast.18, ...), custom_call_target="tpu_custom_call" | custom-call | tf_op jit(solution)/shard_map/own_products/pallas_call | solution.py:125
  63.9 0.0 copy-done
  64.0 3.9 %collective-permute-done.other.rows_in.rows_cot = bf16[1024,2048]{1,0:T(8,128)(2,1)S(1)} collective-permute-done((bf16[1024,2048]{1,0:T(8,128)(2,1)S(1)}, bf16[1024,2048]{1,0:T(8,128)(2,1)S(1)}, u32[]{:S(2)}, u32[]{:S(2)}) %collective-permute-start) | collective-permute-done | bytes 4194336 | tf_op jit(solution)/shard_map/ppermute | solution.py:30
  67.9 5.2 %other_products.1 = (bf16[1024,384]{1,0:T(8,128)(2,1)S(1)}, bf16[1024,768]{1,0:T(8,128)(2,1)S(1)}, bf16[1024,1024]{1,0:T(8,128)(2,1)S(1)}) custom-call(bf16[1024,2048]{1,0:T(8,128)(2,1)S(1)} %collective-permute-done.other.rows_in.rows_cot, f32[1024,768]{1,0:T(8,128)S(1)} %get-tuple-element.51.first_part, f32[1024,384]{1,0:T(8,128)S(1)} %get-tuple-element.52.cot_part, ...), custom_call_target="tpu_custom_call" | custom-call | tf_op jit(solution)/shard_map/other_products/pallas_call | solution.py:164
  73.1 0.4 collective-permute-start.1
  73.5 1.8 kept_half.1
  75.3 0.0 copy-done.2
  75.3 0.0 copy-start.3
  75.4 0.9 copy-done.3
  76.2 1.3 collective-permute-done.1.received
  77.5 0.5 pair_sum.1
  78.0 31.6 %all_to_all.31 = bf16[16,64,1024]{2,1,0:T(8,128)(2,1)S(1)} all-to-all(bf16[16,64,1024]{2,1,0:T(8,128)(2,1)S(1)} %bitcast.21), channel_id=1, replica_groups=mesh['sp'=16,'tp'=16] {'sp'}, dimensions={0} | all-to-all | bytes 4194304 | tf_op jit(solution)/shard_map/all_to_all | solution.py:25
  109.7 0.8 combine.1
  110.4 24.7 %all_to_all.32.pieces = bf16[8,256,128]{2,1,0:T(8,128)(2,1)S(1)} all-to-all(bf16[8,256,128]{2,1,0:T(8,128)(2,1)S(1)} %combine.1), channel_id=1, replica_groups={{0,2,4,6,8,10,12,14},{1,3,5,7,9,11,13,15},{16,18,20,22,24,26,28,30},{17..., dimensions={0} | all-to-all | bytes 1048576 | tf_op jit(solution)/shard_map/all_to_all | solution.py:25
  135.2 0.0 copy-start.14
  135.2 0.0 copy-start.15
  135.2 0.2 mix.1
  135.3 18.1 %all_to_all.33.mixed = bf16[8,256,128]{2,1,0:T(8,128)(2,1)S(1)} all-to-all(bf16[8,256,128]{2,1,0:T(8,128)(2,1)S(1)} %mix.1), channel_id=1, replica_groups={{0,2,4,6,8,10,12,14},{1,3,5,7,9,11,13,15},{16,18,20,22,24,26,28,30},{17..., dimensions={0} | all-to-all | bytes 1048576 | tf_op jit(solution)/shard_map/all_to_all | solution.py:25
  153.4 0.0 collective-permute-start.2
  153.4 0.0 copy-done.9
  153.5 0.5 own_mixed.1
  153.9 1.4 collective-permute-done.2.mixed
  155.3 1.0 norm_cot.1
  156.3 3.5 %all-to-all-start.4 = ((f32[16,2,256]{2,1,0:T(2,128)}), f32[16,2,256]{2,1,0:T(2,128)S(1)}, u32[]{:S(2)}, u32[]{:S(2)}) async-start(f32[16,2,256]{2,1,0:T(2,128)} %get-tuple-element.62), calls=%async_computation.4 | async-start | bytes 65536 | tf_op jit(solution)/shard_map/all_to_all | solution.py:25
  159.8 1.2 proj_parts.1
  161.0 6.5 %all-to-all-done.4.sums = f32[16,2,256]{2,1,0:T(2,128)S(1)} async-done(((f32[16,2,256]{2,1,0:T(2,128)}), f32[16,2,256]{2,1,0:T(2,128)S(1)}, u32[]{:S(2)}, u32[]{:S(2)}) %all-to-all-start.4) | async-done | bytes 32800 | tf_op jit(solution)/shard_map/all_to_all | solution.py:25
  167.5 6.5 %all-to-all-start.5 = ((bf16[16,128,128]{2,1,0:T(8,128)(2,1)}), bf16[16,128,128]{2,1,0:T(8,128)(2,1)S(1)}, u32[]{:S(2)}, u32[]{:S(2)}) async-start(bf16[16,128,128]{2,1,0:T(8,128)(2,1)} %proj_parts.1), calls=%async_computation.5 | async-start | bytes 1048576 | tf_op jit(solution)/shard_map/all_to_all | solution.py:25
  174.0 6.7 %own_grads.1 = (bf16[2048,384]{1,0:T(8,128)(2,1)}, bf16[2048,384]{1,0:T(8,128)(2,1)}, bf16[384,2048]{1,0:T(8,128)(2,1)}) custom-call(s32[1]{0:T(128)} %bitcast.core, bf16[1024,2048]{1,0:T(8,128)(2,1)} %bitcast.19, bf16[1024,2048]{1,0:T(8,128)(2,1)} %bitcast.20, bf16[384,1024]{1,0:T(8,128)(2,1)} %copy-done.3, bf16[1024,768]{1,0:T(8,128)(2,1)} %copy-done.2), custom_call_target="tpu_custom_call" | custom-call | tf_op jit(solution)/shard_map/own_grads/pallas_call | solution.py:232
  180.6 0.1 conv_cot.1
  180.8 4.9 %collective-permute-start.3 = (f32[32,128]{1,0:T(8,128)S(1)}, f32[32,128]{1,0:T(8,128)S(1)}, u32[]{:S(2)}, u32[]{:S(2)}) collective-permute-start(f32[32,128]{1,0:T(8,128)S(1)} %get-tuple-element.83), channel_id=1, source_target_pairs={{16,0},{32,16},{48,32},{64,48},{80,64},{96,80},{112,96},{128,112},... | collective-permute-start | bytes 49160 | tf_op jit(solution)/shard_map/ppermute | solution.py:547
  185.6 0.0 copy-start.10
  185.7 0.0 copy-start.11
  185.7 0.0 copy-start.12
  185.7 6.7 %other_grads.1 = (bf16[2048,384]{1,0:T(8,128)(2,1)}, bf16[2048,384]{1,0:T(8,128)(2,1)}, bf16[384,2048]{1,0:T(8,128)(2,1)}) custom-call(s32[1]{0:T(128)} %bitcast.core, bf16[1024,2048]{1,0:T(8,128)(2,1)} %copy-done.1, bf16[1024,2048]{1,0:T(8,128)(2,1)} %copy-done.1, ...), custom_call_target="tpu_custom_call", output_to_operand_aliasing={{0}: (5, {}), {1}: (6, {}), {2}: (7, {})} | custom-call | tf_op jit(solution)/shard_map/other_grads/pallas_call | solution.py:232
  192.4 0.0 collective-permute-done.3.rim
  192.4 1.0 glu_cot.1
  193.4 0.0 all-to-all-done.5.parts
  193.4 0.8 proj_sum.1
  (18 shorter events, 0.0 us)
Async XLA Ops:
  4.9 55.8 %copy-start.6 = (bf16[1,2048,384]{2,1,0:T(8,128)(2,1)S(1)}, bf16[1,2048,384]{2,1,0:T(8,128)(2,1)}, u32[]{:S(2)}) copy-start(bf16[1,2048,384]{2,1,0:T(8,128)(2,1)} %param.19) | copy-start | bytes 4718596
  4.9 55.8 %copy-start.7 = (bf16[1,2048,384]{2,1,0:T(8,128)(2,1)S(1)}, bf16[1,2048,384]{2,1,0:T(8,128)(2,1)}, u32[]{:S(2)}) copy-start(bf16[1,2048,384]{2,1,0:T(8,128)(2,1)} %param.20) | copy-start | bytes 4718596
  4.9 55.8 %copy-start.8 = (bf16[1,384,2048]{2,1,0:T(8,128)(2,1)S(1)}, bf16[1,384,2048]{2,1,0:T(8,128)(2,1)}, u32[]{:S(2)}) copy-start(bf16[1,384,2048]{2,1,0:T(8,128)(2,1)} %param.21) | copy-start | bytes 4718596
  60.7 3.2 %copy-start = (bf16[16,64,2048]{2,1,0:T(8,128)(2,1)}, bf16[16,64,2048]{2,1,0:T(8,128)(2,1)S(1)}, u32[]{:S(2)}) copy-start(bf16[16,64,2048]{2,1,0:T(8,128)(2,1)S(1)} %all_to_all.30) | copy-start | bytes 12582916
  60.7 7.2 %collective-permute-start = (bf16[1024,2048]{1,0:T(8,128)(2,1)S(1)}, bf16[1024,2048]{1,0:T(8,128)(2,1)S(1)}, u32[]{:S(2)}, u32[]{:S(2)}) collective-permute-start(bf16[1024,2048]{1,0:T(8,128)(2,1)S(1)} %bitcast.17), channel_id=1, source_target_pairs={{0,1},{1,0},{2,3},{3,2},{4,5},{5,4},{6,7},{7,6},{8,9},{9,8},{10,11... | collective-permute-start | bytes 12582920 | tf_op jit(solution)/shard_map/ppermute | solution.py:30
  67.9 5.2 %copy-start.1 = (bf16[1024,2048]{1,0:T(8,128)(2,1)}, bf16[1024,2048]{1,0:T(8,128)(2,1)S(1)}, u32[]{:S(2)}) copy-start(bf16[1024,2048]{1,0:T(8,128)(2,1)S(1)} %collective-permute-done.other.rows_in.rows_cot) | copy-start | bytes 12582916
  73.1 2.2 %copy-start.2 = (bf16[1024,768]{1,0:T(8,128)(2,1)}, bf16[1024,768]{1,0:T(8,128)(2,1)S(1)}, u32[]{:S(2)}) copy-start(bf16[1024,768]{1,0:T(8,128)(2,1)S(1)} %get-tuple-element.66.cots) | copy-start | bytes 4718596
  73.1 4.4 %collective-permute-start.1 = (bf16[1024,1024]{1,0:T(8,128)(2,1)S(1)}, bf16[1024,1024]{1,0:T(8,128)(2,1)S(1)}, u32[]{:S(2)}, u32[]{:S(2)}) collective-permute-start(bf16[1024,1024]{1,0:T(8,128)(2,1)S(1)} %get-tuple-element.60), channel_id=1, source_target_pairs={{0,1},{1,0},{2,3},{3,2},{4,5},{5,4},{6,7},{7,6},{8,9},{9,8},{10,11... | collective-permute-start | bytes 6291464 | tf_op jit(solution)/shard_map/ppermute | solution.py:30
  75.3 0.9 copy-start.3
  109.7 25.5 %copy-start.4 = (bf16[256,2048]{1,0:T(8,128)(2,1)S(1)}, bf16[256,2048]{1,0:T(8,128)(2,1)}, u32[]{:S(2)}) copy-start(bf16[256,2048]{1,0:T(8,128)(2,1)} %cotangent.1) | copy-start | bytes 3145732
  135.1 18.3 %copy-start.5 = (bf16[2048,128]{1,0:T(8,128)(2,1)S(1)}, bf16[2048,128]{1,0:T(8,128)(2,1)}, u32[]{:S(2)}) copy-start(bf16[2048,128]{1,0:T(8,128)(2,1)} %w_out.3) | copy-start | bytes 1572868
  135.2 18.3 %copy-start.9 = (bf16[128,256]{1,0:T(8,128)(2,1)S(1)}, bf16[128,256]{1,0:T(8,128)(2,1)}, u32[]{:S(2)}) copy-start(bf16[128,256]{1,0:T(8,128)(2,1)} %conv_out.7) | copy-start | bytes 196612
  135.2 18.3 %copy-start.13 = (f32[256]{0:T(256)S(1)}, f32[256]{0:T(256)}, u32[]{:S(2)}) copy-start(f32[256]{0:T(256)} %param.28) | copy-start | bytes 3076
  135.2 18.3 %copy-start.14 = (f32[256]{0:T(256)S(1)}, f32[256]{0:T(256)}, u32[]{:S(2)}) copy-start(f32[256]{0:T(256)} %param.29) | copy-start | bytes 3076
  135.2 18.3 %copy-start.15 = (f32[128]{0:T(128)S(1)}, f32[128]{0:T(128)}, u32[]{:S(2)}) copy-start(f32[128]{0:T(128)} %param.23) | copy-start | bytes 1540
  153.4 1.9 collective-permute-start.2
  156.3 11.2 %all-to-all-start.4 = ((f32[16,2,256]{2,1,0:T(2,128)}), f32[16,2,256]{2,1,0:T(2,128)S(1)}, u32[]{:S(2)}, u32[]{:S(2)}) async-start(f32[16,2,256]{2,1,0:T(2,128)} %get-tuple-element.62), calls=%async_computation.4 | async-start | bytes 65536 | tf_op jit(solution)/shard_map/all_to_all | solution.py:25
  167.5 25.9 %all-to-all-start.5 = ((bf16[16,128,128]{2,1,0:T(8,128)(2,1)}), bf16[16,128,128]{2,1,0:T(8,128)(2,1)S(1)}, u32[]{:S(2)}, u32[]{:S(2)}) async-start(bf16[16,128,128]{2,1,0:T(8,128)(2,1)} %proj_parts.1), calls=%async_computation.5 | async-start | bytes 1048576 | tf_op jit(solution)/shard_map/all_to_all | solution.py:25
  180.8 11.6 %collective-permute-start.3 = (f32[32,128]{1,0:T(8,128)S(1)}, f32[32,128]{1,0:T(8,128)S(1)}, u32[]{:S(2)}, u32[]{:S(2)}) collective-permute-start(f32[32,128]{1,0:T(8,128)S(1)} %get-tuple-element.83), channel_id=1, source_target_pairs={{16,0},{32,16},{48,32},{64,48},{80,64},{96,80},{112,96},{128,112},... | collective-permute-start | bytes 49160 | tf_op jit(solution)/shard_map/ppermute | solution.py:547
  185.6 6.7 %copy-start.10 = (bf16[128,256]{1,0:T(8,128)(2,1)S(1)}, bf16[128,256]{1,0:T(8,128)(2,1)}, u32[]{:S(2)}) copy-start(bf16[128,256]{1,0:T(8,128)(2,1)} %glu_value.1) | copy-start | bytes 196612
  185.7 6.7 %copy-start.11 = (bf16[128,256]{1,0:T(8,128)(2,1)S(1)}, bf16[128,256]{1,0:T(8,128)(2,1)}, u32[]{:S(2)}) copy-start(bf16[128,256]{1,0:T(8,128)(2,1)} %glu_gate.1) | copy-start | bytes 196612
  185.7 6.7 %copy-start.12 = (f32[31,128]{1,0:T(8,128)S(1)}, f32[31,128]{1,0:T(8,128)}, u32[]{:S(2)}) copy-start(f32[31,128]{1,0:T(8,128)} %taps.1) | copy-start | bytes 47620
